TPU v7x, 512 devices: a whole 4x8x8 slice. The times are simulated.
512 devices in a mesh: fs: 128 (over z, y, core), tp: 4 (over x).
Axes of the slice: x: 4, y: 8, z: 8, core: 2. Of those that a mesh axis runs over, the one named last changes fastest.
Arguments:
- query_one: bfloat16 [81920, 1024], P('fs', 'tp'), as said below
- key_one: bfloat16 [81920, 1024], P('fs', 'tp'), as said below
- query_two: bfloat16 [81920, 1024], P('fs', 'tp'), as said below
- key_two: bfloat16 [81920, 1024], P('fs', 'tp'), as said below
- values: bfloat16 [81920, 2048], P('fs', 'tp'), may hold values from -6 to 6
- mix_ratio: float32 [8], P('tp'), may hold values from 0.3 to 0.8
- head_gain: float32 [256], replicated, may hold values from 0.1 to 1.9
- cotangent: bfloat16 [81920, 2048], P('fs', 'tp'), may hold values from -0.1875 to 0.1875
- left_roots: bfloat16 [2048, 2048], P('fs'), as said below
- right_roots: bfloat16 [2048, 256], P('tp'), as said below
- weight: float32 [2048, 2048], P('fs', 'tp'), may hold values from -3 to 3
- momentum: float32 [2048, 2048], P('fs', 'tp'), as said below
Outputs:
- update_step: float32 [2048, 2048], P('fs', 'tp')
- weight_new: float32 [2048, 2048], P('fs', 'tp')
- momentum_new: float32 [2048, 2048], P('fs', 'tp')
- weight_copy: bfloat16 [2048, 2048], P(None, 'tp')
Inputs may be any that keep to these rules, and one draw needn't show every extreme that they name: `query_one`: Real-valued. `key_one`: Real-valued. `query_two`: Real-valued. `key_two`: Real-valued. `left_roots`: Real-valued. `right_roots`: Real-valued. `momentum`: Real-valued.
All inputs are finite; a program needn't handle non-finite values.
Results may differ from a plain program's by a relative error of at most 0.0039.
Values may be sent and summed in bfloat16 or wider, within the bound.
A program may use at most 64 MiB of HBM per device.

v0:
```python
import jax
import jax.numpy as jnp
from jax import lax
from jax.sharding import Mesh
from jax.sharding import PartitionSpec as P

D = 2048
HV = 2048
FS = ("fs_0", "fs_1", "fs_2")


epsilon = 1e-06
momentum_decay = 0.8
clip_level = 0.5
weight_decay = 0.2
step_rate = 0.1


def laid_out(blocks, dim):
    shape = list(blocks.shape[1:])
    shape[dim] *= blocks.shape[0]
    return jnp.moveaxis(blocks, 0, dim).reshape(shape)


def from_everyone(shard, axis):
    length = lax.axis_size(axis)
    return lax.all_to_all(
        jnp.broadcast_to(shard[None], (length, *shard.shape)), axis, 0, 0, tiled=True
    )


def gather_directly(shard, axis, dim):
    return laid_out(from_everyone(shard, axis), dim)


def in_blocks(shard, dim, length):
    before, after = (shard.shape[:dim], shard.shape[dim + 1 :])
    return jnp.moveaxis(shard.reshape(*before, length, -1, *after), dim, 0)


def sum_at_owner(shard, axis, dim):
    length = lax.axis_size(axis)
    blocks = lax.all_to_all(in_blocks(shard, dim, length), axis, 0, 0, tiled=True)
    return jnp.sum(blocks.astype(jnp.float32), axis=0)


def summed_rows(shard, axes, dim):
    far, near = axes
    own = sum_at_owner(in_blocks(shard, dim, lax.axis_size(far)), near, dim + 1)
    return jnp.sum(
        lax.all_to_all(own.astype(jnp.bfloat16), far, 0, 0, tiled=True).astype(jnp.float32), axis=0
    )


def from_partner(block, axis, apart):
    count = lax.axis_size(axis)
    route = []
    for low in range(count):
        high = low | 1 << apart
        if high != low and high < count:
            route += [(low, high), (high, low)]
    return lax.ppermute(block, axis, route)


def taken_together(shard, axis):
    return from_everyone(shard, axis).sum(axis=0)


def one_axis_at_a_time(shard, axes):
    far, near = axes
    nearer = taken_together(shard, near)
    return taken_together(nearer, far)


def gather_axes(shard, axes, dim):
    far, near = axes
    blocks = from_everyone(from_everyone(shard, far), near)
    return laid_out(blocks.swapaxes(0, 1).reshape(-1, *shard.shape), dim)


def local(
    query_one,
    key_one,
    query_two,
    key_two,
    values,
    mix_ratio,
    head_gain,
    cotangent,
    left_roots,
    right_roots,
    weight,
    momentum,
):
    local_heads = mix_ratio.shape[0]
    tok_rows = query_one.shape[0]
    key_width = query_one.shape[1] // local_heads
    value_width = values.shape[1] // local_heads
    causal = jnp.tril(jnp.ones((tok_rows, tok_rows), dtype=bool))

    def probs(query, keys):
        scores = jnp.einsum(
            "qhd,khd->hqk",
            query.reshape(tok_rows, local_heads, key_width),
            keys.reshape(tok_rows, local_heads, key_width),
            preferred_element_type=jnp.float32,
        ) * key_width ** (-0.5)
        return jax.nn.softmax(jnp.where(causal, scores, -jnp.inf), axis=-1)

    mixed = (
        probs(query_one, key_one) - mix_ratio[:, None, None] * probs(query_two, key_two)
    ).astype(jnp.bfloat16)
    head_out = jnp.einsum(
        "hqk,khd->qhd",
        mixed,
        values.reshape(tok_rows, local_heads, value_width),
        preferred_element_type=jnp.float32,
    )
    square = jnp.mean(head_out * head_out, axis=-1, keepdims=True)
    attended = (head_out * lax.rsqrt(square + epsilon) * head_gain).astype(jnp.bfloat16)
    attended = attended.reshape(tok_rows, local_heads * value_width)
    whole_cot = gather_directly(cotangent, "tp", 1)
    model_width = whole_cot.shape[1]
    own_rows = weight.shape[0]
    own_cols = weight.shape[1]
    contract = (((0,), (0,)), ((), ()))
    right_full = right_roots.astype(jnp.float32).reshape(local_heads, value_width, value_width)
    left_rows = left_roots.astype(jnp.float32)
    summed = summed_rows(
        lax.dot_general(whole_cot, attended, contract, preferred_element_type=jnp.float32).astype(
            jnp.bfloat16
        ),
        (("fs_0", "fs_1"), "fs_2"),
        0,
    )
    position = lax.axis_index(FS)
    bit_count = (model_width // own_rows).bit_length() - 1
    assembled = summed
    for bit in range(bit_count):
        other = from_partner(assembled.astype(jnp.bfloat16), FS, bit).astype(assembled.dtype)
        upper = position // 2**bit % 2 == 1
        assembled = jnp.where(
            upper,
            jnp.concatenate([other, assembled], axis=0),
            jnp.concatenate([assembled, other], axis=0),
        )
    left_done = jnp.dot(
        left_rows, assembled, precision=lax.Precision.HIGHEST, preferred_element_type=jnp.float32
    )
    shaped = left_done.reshape(own_rows, local_heads, value_width)
    preconditioned = jnp.einsum(
        "dhc,hce->dhe", shaped, right_full, precision=lax.Precision.HIGHEST
    ).reshape(own_rows, own_cols)
    momentum_new = momentum_decay * momentum + (1.0 - momentum_decay) * preconditioned
    total = one_axis_at_a_time(
        jnp.sum(momentum_new * momentum_new), (("fs_0", "fs_1"), ("fs_2", "tp"))
    )
    factor = clip_level * lax.rsqrt(total / (D * HV) + epsilon)
    update_step = factor * momentum_new + weight_decay * weight
    weight_new = weight - step_rate * update_step
    weight_copy = gather_axes(weight_new.astype(jnp.bfloat16), (("fs_0", "fs_1"), "fs_2"), 0)
    return (update_step, weight_new, momentum_new, weight_copy)


def solution(mesh):
    split = Mesh(mesh.devices.reshape(8, 8, 2, mesh.shape["tp"]), ("fs_0", "fs_1", "fs_2", "tp"))
    return jax.shard_map(
        local,
        mesh=split,
        in_specs=(
            P(FS, "tp"),
            P(FS, "tp"),
            P(FS, "tp"),
            P(FS, "tp"),
            P(FS, "tp"),
            P("tp"),
            P(),
            P(FS, "tp"),
            P(FS, None),
            P("tp", None),
            P(FS, "tp"),
            P(FS, "tp"),
        ),
        out_specs=(P(FS, "tp"), P(FS, "tp"), P(FS, "tp"), P(None, "tp")),
        check_vma=False,
    )
```

profile of v0, /device:TPU:1, one launch (start us, length us, event | category | flops | bytes accessed | tf_op | source)
XLA Modules:
  0.0 289.5 jit_solution(11532097894610682174)
XLA Ops:
  0.6 0.0 copy-start
  0.6 1.4 copy.74
  2.1 1.8 broadcast_in_dim.26
  3.8 4.8 %all-to-all-start = ((bf16[4,640,512]{1,2,0:T(8,128)(2,1)}), bf16[4,640,512]{1,2,0:T(8,128)(2,1)S(1)}, u32[]{:S(2)}, u32[]{:S(2)}) async-start(bf16[4,640,512]{1,2,0:T(8,128)(2,1)} %broadcast_in_dim.26), calls=%async_computation | async-start | bytes 5242880 | tf_op jit(solution)/shard_map/all_to_all | solution.py:27
  8.7 2.2 copy.83
  10.9 0.1 iota_compare_fusion
  11.0 0.0 copy-done
  11.0 1.6 fusion.29
  12.6 0.0 copy-done.1
  12.6 0.0 copy-done.2
  12.6 2.3 fusion.24
  14.9 3.3 %fusion.49 = (f32[2,640]{1,0:T(2,128)S(1)}, f32[2,640,640]{1,2,0:T(8,128)}) fusion(f32[2,640,640]{1,2,0:T(8,128)S(1)} %fusion.29, pred[640,640]{0,1:T(8,128)(4,1)S(1)} %iota_compare_fusion), kind=kOutput, calls=%fused_computation.72 | output fusion | flops 4915839 | bytes 6968320 | tf_op jit(solution)/shard_map/sub | solution.py:108
  18.2 0.0 copy-done.9
  18.2 7.6 %multiply_reduce_fusion = (f32[640,2]{0,1:T(2,128)S(1)}, f32[640,2,256]{0,2,1:T(8,128)}) fusion(bf16[640,2,256]{0,2,1:T(8,128)(2,1)} %bitcast.61, f32[2,640,640]{1,2,0:T(8,128)} %get-tuple-element.22, f32[2]{0:T(128)S(1)} %copy-done.9, f32[2,640]{1,0:T(2,128)S(1)} %get-tuple-element.21, f32[2,640,640]{1,2,0:T(8,128)} %fusion.24, ...), kind=kOutput, calls=%fused_computation.34 | convolution fusion | flops 428280320 | bytes 8939528 | tf_op jit(solution)/shard_map/hqk,khd->qhd/dot_general | solution.py:113
  25.9 0.0 copy-done.7
  25.9 2.3 multiply_convert_fusion
  28.2 6.9 %all-to-all-done = bf16[4,640,512]{1,2,0:T(8,128)(2,1)S(1)} async-done(((bf16[4,640,512]{1,2,0:T(8,128)(2,1)}), bf16[4,640,512]{1,2,0:T(8,128)(2,1)S(1)}, u32[]{:S(2)}, u32[]{:S(2)}) %all-to-all-start) | async-done | bytes 2621472 | tf_op jit(solution)/shard_map/all_to_all | solution.py:27
  35.1 4.2 %fusion.9 = bf16[2048,512]{0,1:T(8,128)(2,1)} fusion(bf16[640,512]{0,1:T(8,128)(2,1)} %bitcast.62, bf16[640,2048]{0,1:T(8,128)(2,1)S(1)} %bitcast.59), kind=kOutput, calls=%fused_computation.16 | convolution fusion | flops 1343225856 | bytes 5373952 | tf_op jit(solution)/shard_map/dot_general | solution.py:130
  39.3 2.9 copy.75
  42.2 0.2 copy.76
  42.4 11.5 %all_to_all.37 = bf16[2,64,16,512]{3,2,1,0:T(8,128)(2,1)S(1)} all-to-all(bf16[2,64,16,512]{3,2,1,0:T(8,128)(2,1)S(1)} %copy.76), channel_id=1, replica_groups=mesh['fs_0'=8,'fs_1'=8,'fs_2'=2,'tp'=4] {'fs_2'}, dimensions={0} | all-to-all | bytes 4194304 | tf_op jit(solution)/shard_map/all_to_all | solution.py:43
  53.9 0.6 reduce_sum.78
  54.5 43.9 %all_to_all.38 = bf16[64,16,512]{2,1,0:T(8,128)(2,1)S(1)} all-to-all(bf16[64,16,512]{2,1,0:T(8,128)(2,1)S(1)} %reduce_sum.78), channel_id=1, replica_groups=mesh['fs_0'=8,'fs_1'=8,'fs_2'=2,'tp'=4] {'fs_0','fs_1'}, dimensions={0} | all-to-all | bytes 2097152 | tf_op jit(solution)/shard_map/all_to_all | solution.py:51
  98.4 0.2 convert_reduce_fusion
  98.5 4.7 %collective-permute-start = (bf16[16,512]{1,0:T(8,128)(2,1)S(1)}, bf16[16,512]{1,0:T(8,128)(2,1)S(1)}, u32[]{:S(2)}, u32[]{:S(2)}) collective-permute-start(bf16[16,512]{1,0:T(8,128)(2,1)S(1)} %convert_element_type.69), channel_id=1, source_target_pairs={{0,4},{4,0},{8,12},{12,8},{16,20},{20,16},{24,28},{28,24},{32,36},... | collective-permute-start | bytes 49160 | tf_op jit(solution)/shard_map/ppermute | solution.py:62
  103.2 0.8 collective-permute-done
  104.1 2.9 %collective-permute-start.1 = (bf16[32,512]{1,0:T(8,128)(2,1)S(1)}, bf16[32,512]{1,0:T(8,128)(2,1)S(1)}, u32[]{:S(2)}, u32[]{:S(2)}) collective-permute-start(bf16[32,512]{1,0:T(8,128)(2,1)S(1)} %get-tuple-element.19), channel_id=1, source_target_pairs={{0,8},{8,0},{4,12},{12,4},{16,24},{24,16},{20,28},{28,20},{32,40},... | collective-permute-start | bytes 98312 | tf_op jit(solution)/shard_map/ppermute | solution.py:62
  107.0 1.7 collective-permute-done.1
  108.7 3.7 %collective-permute-start.2 = (bf16[64,512]{1,0:T(8,128)(2,1)S(1)}, bf16[64,512]{1,0:T(8,128)(2,1)S(1)}, u32[]{:S(2)}, u32[]{:S(2)}) collective-permute-start(bf16[64,512]{1,0:T(8,128)(2,1)S(1)} %get-tuple-element.17), channel_id=1, source_target_pairs={{0,16},{16,0},{4,20},{20,4},{8,24},{24,8},{12,28},{28,12},{32,48},... | collective-permute-start | bytes 196616 | tf_op jit(solution)/shard_map/ppermute | solution.py:62
  112.4 2.2 collective-permute-done.2
  114.7 5.7 %collective-permute-start.3 = (bf16[128,512]{1,0:T(8,128)(2,1)S(1)}, bf16[128,512]{1,0:T(8,128)(2,1)S(1)}, u32[]{:S(2)}, u32[]{:S(2)}) collective-permute-start(bf16[128,512]{1,0:T(8,128)(2,1)S(1)} %get-tuple-element.15), channel_id=1, source_target_pairs={{0,32},{32,0},{4,36},{36,4},{8,40},{40,8},{12,44},{44,12},{16,48},... | collective-permute-start | bytes 393224 | tf_op jit(solution)/shard_map/ppermute | solution.py:62
  120.4 5.3 %collective-permute-done.3 = bf16[128,512]{1,0:T(8,128)(2,1)S(1)} collective-permute-done((bf16[128,512]{1,0:T(8,128)(2,1)S(1)}, bf16[128,512]{1,0:T(8,128)(2,1)S(1)}, u32[]{:S(2)}, u32[]{:S(2)}) %collective-permute-start.3) | collective-permute-done | bytes 131104 | tf_op jit(solution)/shard_map/ppermute | solution.py:62
  125.8 0.1 fusion.45
  125.9 1.9 collective-permute-start.4
  127.8 5.2 %collective-permute-done.4 = bf16[256,512]{1,0:T(8,128)(2,1)S(1)} collective-permute-done((bf16[256,512]{1,0:T(8,128)(2,1)S(1)}, bf16[256,512]{1,0:T(8,128)(2,1)S(1)}, u32[]{:S(2)}, u32[]{:S(2)}) %collective-permute-start.4) | collective-permute-done | bytes 262176 | tf_op jit(solution)/shard_map/ppermute | solution.py:62
  133.0 0.1 convert_element_type.78
  133.1 0.2 fusion.44
  133.3 3.5 %collective-permute-start.5 = (bf16[512,512]{1,0:T(8,128)(2,1)S(1)}, bf16[512,512]{1,0:T(8,128)(2,1)S(1)}, u32[]{:S(2)}, u32[]{:S(2)}) collective-permute-start(bf16[512,512]{1,0:T(8,128)(2,1)S(1)} %get-tuple-element.11), channel_id=1, source_target_pairs={{0,128},{128,0},{4,132},{132,4},{8,136},{136,8},{12,140},{140,12},... | collective-permute-start | bytes 1572872 | tf_op jit(solution)/shard_map/ppermute | solution.py:62
  136.8 23.7 %collective-permute-done.5 = bf16[512,512]{1,0:T(8,128)(2,1)S(1)} collective-permute-done((bf16[512,512]{1,0:T(8,128)(2,1)S(1)}, bf16[512,512]{1,0:T(8,128)(2,1)S(1)}, u32[]{:S(2)}, u32[]{:S(2)}) %collective-permute-start.5) | collective-permute-done | bytes 524320 | tf_op jit(solution)/shard_map/ppermute | solution.py:62
  160.5 0.1 convert_element_type.80
  160.6 0.0 copy-start.8
  160.6 1.4 fusion.43
  162.0 4.0 %collective-permute-start.6 = (bf16[1024,512]{1,0:T(8,128)(2,1)}, bf16[1024,512]{1,0:T(8,128)(2,1)S(1)}, u32[]{:S(2)}, u32[]{:S(2)}) collective-permute-start(bf16[1024,512]{1,0:T(8,128)(2,1)} %get-tuple-element.9), channel_id=1, source_target_pairs={{0,256},{256,0},{4,260},{260,4},{8,264},{264,8},{12,268},{268,12},... | collective-permute-start | bytes 3145736 | tf_op jit(solution)/shard_map/ppermute | solution.py:62
  166.1 48.3 %collective-permute-done.6 = bf16[1024,512]{1,0:T(8,128)(2,1)S(1)} collective-permute-done((bf16[1024,512]{1,0:T(8,128)(2,1)}, bf16[1024,512]{1,0:T(8,128)(2,1)S(1)}, u32[]{:S(2)}, u32[]{:S(2)}) %collective-permute-start.6) | collective-permute-done | bytes 1048608 | tf_op jit(solution)/shard_map/ppermute | solution.py:62
  214.4 0.3 convert_element_type.82
  214.7 0.0 copy-done.8
  214.7 0.0 copy-start.3
  214.8 0.0 copy-start.5
  214.8 0.0 copy-start.6
  214.8 1.8 fusion.3
  216.6 0.2 fusion.23
  216.8 0.6 multiply_reduce_fusion.1
  217.4 0.7 broadcast_in_dim.27
  218.1 7.4 %all_to_all.39 = f32[8,1,1]{2,1,0:T(1,128)S(1)} all-to-all(f32[8,1,1]{2,1,0:T(1,128)S(1)} %broadcast_in_dim.27), channel_id=1, replica_groups=mesh['fs_0'=8,'fs_1'=8,'fs_2'=2,'tp'=4] {'fs_2','tp'}, dimensions={0} | all-to-all | bytes 64 | tf_op jit(solution)/shard_map/all_to_all | solution.py:27
  225.5 0.6 reduce_sum.81
  226.1 0.7 broadcast_in_dim.28
  226.8 19.0 %all_to_all.40 = f32[64,1,1]{2,1,0:T(1,128)S(1)} all-to-all(f32[64,1,1]{2,1,0:T(1,128)S(1)} %broadcast_in_dim.28), channel_id=1, replica_groups=mesh['fs_0'=8,'fs_1'=8,'fs_2'=2,'tp'=4] {'fs_0','fs_1'}, dimensions={0} | all-to-all | bytes 512 | tf_op jit(solution)/shard_map/all_to_all | solution.py:27
  245.8 0.7 reduce_sum.82
  247.2 0.6 fusion.42
  247.8 0.1 broadcast_in_dim.29
  248.0 29.7 %all_to_all.41 = bf16[64,16,512]{2,1,0:T(8,128)(2,1)S(1)} all-to-all(bf16[64,16,512]{2,1,0:T(8,128)(2,1)S(1)} %broadcast_in_dim.29), channel_id=1, replica_groups=mesh['fs_0'=8,'fs_1'=8,'fs_2'=2,'tp'=4] {'fs_0','fs_1'}, dimensions={0} | all-to-all | bytes 2097152 | tf_op jit(solution)/shard_map/all_to_all | solution.py:27
  277.7 0.3 broadcast_in_dim.30
  278.0 10.0 %all_to_all.42 = bf16[2,64,16,512]{3,2,1,0:T(8,128)(2,1)S(1)} all-to-all(bf16[2,64,16,512]{3,2,1,0:T(8,128)(2,1)S(1)} %broadcast_in_dim.30), channel_id=1, replica_groups=mesh['fs_0'=8,'fs_1'=8,'fs_2'=2,'tp'=4] {'fs_2'}, dimensions={0} | all-to-all | bytes 4194304 | tf_op jit(solution)/shard_map/all_to_all | solution.py:27
  287.9 1.5 copy.81
  (19 shorter events, 0.1 us)
Async XLA Ops:
  0.6 10.4 %copy-start = (bf16[640,256]{1,0:T(8,128)(2,1)S(1)}, bf16[640,256]{1,0:T(8,128)(2,1)}, u32[]{:S(2)}) copy-start(bf16[640,256]{1,0:T(8,128)(2,1)} %param.13) | copy-start | bytes 983044
  3.8 31.2 %all-to-all-start = ((bf16[4,640,512]{1,2,0:T(8,128)(2,1)}), bf16[4,640,512]{1,2,0:T(8,128)(2,1)S(1)}, u32[]{:S(2)}, u32[]{:S(2)}) async-start(bf16[4,640,512]{1,2,0:T(8,128)(2,1)} %broadcast_in_dim.26), calls=%async_computation | async-start | bytes 5242880 | tf_op jit(solution)/shard_map/all_to_all | solution.py:27
  10.9 1.8 copy-start.1
  10.9 1.8 copy-start.2
  14.9 3.3 %copy-start.9 = (f32[2]{0:T(128)S(1)}, f32[2]{0:T(128)}, u32[]{:S(2)}) copy-start(f32[2]{0:T(128)} %param.17) | copy-start | bytes 28
  18.2 7.7 %copy-start.7 = (f32[256]{0:T(256)S(1)}, f32[256]{0:T(256)}, u32[]{:S(2)}) copy-start(f32[256]{0:T(256)} %param.18) | copy-start | bytes 3076
  98.5 5.5 %collective-permute-start = (bf16[16,512]{1,0:T(8,128)(2,1)S(1)}, bf16[16,512]{1,0:T(8,128)(2,1)S(1)}, u32[]{:S(2)}, u32[]{:S(2)}) collective-permute-start(bf16[16,512]{1,0:T(8,128)(2,1)S(1)} %convert_element_type.69), channel_id=1, source_target_pairs={{0,4},{4,0},{8,12},{12,8},{16,20},{20,16},{24,28},{28,24},{32,36},... | collective-permute-start | bytes 49160 | tf_op jit(solution)/shard_map/ppermute | solution.py:62
  104.1 4.7 %collective-permute-start.1 = (bf16[32,512]{1,0:T(8,128)(2,1)S(1)}, bf16[32,512]{1,0:T(8,128)(2,1)S(1)}, u32[]{:S(2)}, u32[]{:S(2)}) collective-permute-start(bf16[32,512]{1,0:T(8,128)(2,1)S(1)} %get-tuple-element.19), channel_id=1, source_target_pairs={{0,8},{8,0},{4,12},{12,4},{16,24},{24,16},{20,28},{28,20},{32,40},... | collective-permute-start | bytes 98312 | tf_op jit(solution)/shard_map/ppermute | solution.py:62
  108.7 5.9 %collective-permute-start.2 = (bf16[64,512]{1,0:T(8,128)(2,1)S(1)}, bf16[64,512]{1,0:T(8,128)(2,1)S(1)}, u32[]{:S(2)}, u32[]{:S(2)}) collective-permute-start(bf16[64,512]{1,0:T(8,128)(2,1)S(1)} %get-tuple-element.17), channel_id=1, source_target_pairs={{0,16},{16,0},{4,20},{20,4},{8,24},{24,8},{12,28},{28,12},{32,48},... | collective-permute-start | bytes 196616 | tf_op jit(solution)/shard_map/ppermute | solution.py:62
  114.7 11.1 %collective-permute-start.3 = (bf16[128,512]{1,0:T(8,128)(2,1)S(1)}, bf16[128,512]{1,0:T(8,128)(2,1)S(1)}, u32[]{:S(2)}, u32[]{:S(2)}) collective-permute-start(bf16[128,512]{1,0:T(8,128)(2,1)S(1)} %get-tuple-element.15), channel_id=1, source_target_pairs={{0,32},{32,0},{4,36},{36,4},{8,40},{40,8},{12,44},{44,12},{16,48},... | collective-permute-start | bytes 393224 | tf_op jit(solution)/shard_map/ppermute | solution.py:62
  125.9 7.1 %collective-permute-start.4 = (bf16[256,512]{1,0:T(8,128)(2,1)S(1)}, bf16[256,512]{1,0:T(8,128)(2,1)S(1)}, u32[]{:S(2)}, u32[]{:S(2)}) collective-permute-start(bf16[256,512]{1,0:T(8,128)(2,1)S(1)} %get-tuple-element.13), channel_id=1, source_target_pairs={{0,64},{64,0},{4,68},{68,4},{8,72},{72,8},{12,76},{76,12},{16,80},... | collective-permute-start | bytes 786440 | tf_op jit(solution)/shard_map/ppermute | solution.py:62
  133.3 27.2 %collective-permute-start.5 = (bf16[512,512]{1,0:T(8,128)(2,1)S(1)}, bf16[512,512]{1,0:T(8,128)(2,1)S(1)}, u32[]{:S(2)}, u32[]{:S(2)}) collective-permute-start(bf16[512,512]{1,0:T(8,128)(2,1)S(1)} %get-tuple-element.11), channel_id=1, source_target_pairs={{0,128},{128,0},{4,132},{132,4},{8,136},{136,8},{12,140},{140,12},... | collective-permute-start | bytes 1572872 | tf_op jit(solution)/shard_map/ppermute | solution.py:62
  160.6 54.1 %copy-start.8 = (bf16[16,2048]{1,0:T(8,128)(2,1)S(1)}, bf16[16,2048]{1,0:T(8,128)(2,1)}, u32[]{:S(2)}) copy-start(bf16[16,2048]{1,0:T(8,128)(2,1)} %param.20) | copy-start | bytes 196612
  162.0 52.4 %collective-permute-start.6 = (bf16[1024,512]{1,0:T(8,128)(2,1)}, bf16[1024,512]{1,0:T(8,128)(2,1)S(1)}, u32[]{:S(2)}, u32[]{:S(2)}) collective-permute-start(bf16[1024,512]{1,0:T(8,128)(2,1)} %get-tuple-element.9), channel_id=1, source_target_pairs={{0,256},{256,0},{4,260},{260,4},{8,264},{264,8},{12,268},{268,12},... | collective-permute-start | bytes 3145736 | tf_op jit(solution)/shard_map/ppermute | solution.py:62
  214.7 1.8 copy-start.3
  214.8 2.1 copy-start.5
  214.8 32.4 %copy-start.6 = (f32[16,512]{1,0:T(8,128)S(1)}, f32[16,512]{1,0:T(8,128)}, u32[]{:S(2)}) copy-start(f32[16,512]{1,0:T(8,128)} %param.22) | copy-start | bytes 98308
  217.4 60.5 %copy-start.4 = (f32[16,512]{1,0:T(8,128)}, f32[16,512]{1,0:T(8,128)S(1)}, u32[]{:S(2)}) copy-start(f32[16,512]{1,0:T(8,128)S(1)} %get-tuple-element.8) | copy-start | bytes 98308
where the time goes:
time: 290 us; the launch traced here: 289 us
  blocking collectives  122 us (42%)
  waiting for transfers between devices  94.1 us (32%)
  starting transfers between devices  31.2 us (11%)
  matrix products  17.8 us (6%)
  local copies, waits for them, and re-layouts  11.7 us (4%)
  other arithmetic  11.2 us (4%)
    ppermute x7, waiting for transfers between devices, from_partner(): return lax.ppermute(block, axis, route)  87.2 us
    all_to_all x4, blocking collectives, from_everyone(): lax.all_to_all(jnp.broadcast_to(shard[None], (length, *shard.shape)), axi...  66.1 us
    all_to_all x1, blocking collectives, summed_rows(): lax.all_to_all(own.astype(jnp.bfloat16), far, 0, 0, tiled=True)  43.9 us
    ppermute x7, starting transfers between devices, from_partner(): return lax.ppermute(block, axis, route)  26.4 us
    all_to_all x1, blocking collectives, sum_at_owner(): lax.all_to_all(in_blocks(shard, dim, length), axis, 0, 0, tiled=True)  11.5 us
    dot_general x1, matrix products, local(): jnp.einsum('hqk,khd->qhd', mixed, values.reshape(tok_rows, local_heads, v...  7.65 us
    all_to_all x1, waiting for transfers between devices, from_everyone(): lax.all_to_all(jnp.broadcast_to(shard[None], (length, *shard.shape)), axi...  6.9 us
  transfers between devices with their start and end apart: 8, of which 8 were waited for; matrix products, arithmetic and copies ran while one was open for 7% of the time, Pallas kernels for 0%

commit v1 on v0

v1 whole, which is shorter than its diff:
```python
import functools

import jax
import jax.numpy as jnp
from jax import lax
from jax.experimental import pallas as pl
from jax.experimental.pallas import tpu as pltpu
from jax.sharding import Mesh
from jax.sharding import PartitionSpec as P

FS = ("fs_0", "fs_1", "fs_2")
MESH_ID = pl.DeviceIdType.MESH

epsilon = 1e-06
momentum_decay = 0.8
clip_level = 0.5
weight_decay = 0.2
step_rate = 0.1

GROUPS = 8
CHUNK = ((0, 1), (2, 3), (0, 2), (1, 3), (2, 0), (3, 1), (0, 2), (1, 3))
NT = (((1,), (1,)), ((), ()))


def dot(left, right, dims=(((1,), (0,)), ((), ()))):
    return lax.dot_general(left, right, dims, preferred_element_type=jnp.float32)


def kernel(
    entries,
    q1, k1, q2, k2, val, mix, gain, cot, left, right, weight, momentum,
    step_out, weight_out, momentum_out, copy_out,
    cm, cp, at_own, at_send, at_part, gsend, rs1, s1b, rs2, gall, wall, ssx, ssb, ssa, ssd,
    x_s, x_r, c_s, c_r, a_s, a_r, r1_s, r1_r, r2_s, r2_r,
    gb_s, gb_r, ga_s, ga_r, gd_s, gd_r, wb_s, wb_r, wa_s, wa_r, wd_s, wd_r,
    sx_s, sx_r, sb_s, sb_r, sa_s, sa_r, sd_s, sd_r,
):
    z, y, c, x = (lax.axis_index(name) for name in (*FS, "tp"))
    n = rs2.shape[0]
    nx = ssx.shape[0]
    other = 1 - c
    a = z * other + y * c
    b = y * other + z * c

    def at_a(p):
        return (p * other + z * c, y * other + p * c, c, x)

    def at_b(p):
        return (z * other + p * c, p * other + y * c, c, x)

    def at_x(p):
        return (z, y, c, p)

    partner = (z, y, other, x)
    pending = []

    def remote(src, dst, send, recv, where):
        return pltpu.make_async_remote_copy(
            src_ref=src, dst_ref=dst, send_sem=send, recv_sem=recv,
            device_id=where, device_id_type=MESH_ID,
        )

    def start(*parts):
        copy = remote(*parts)
        copy.start()
        pending.append(copy)

    def arrived(dst, send, recv):
        remote(dst, dst, send, recv, partner).wait_recv()

    def around(p, size):
        return lax.rem(p + size, size)

    barrier = pltpu.get_barrier_semaphore()
    peers = [partner]
    for d in range(1, n):
        peers += [at_a(around(a + d, n)), at_b(around(b + d, n))]
    for d in range(1, nx):
        peers.append(at_x(around(x + d, nx)))
    for peer in peers:
        pl.semaphore_signal(barrier, inc=1, device_id=peer, device_id_type=MESH_ID)
    pl.semaphore_wait(barrier, len(peers))

    tokens = cot.shape[0]
    ch = cot.shape[1] // 4
    ahead = at_x(around(x + 1, nx))
    behind = at_x(around(x - 1, nx))

    def half(i):
        return pl.ds(i * ch, ch)

    for g in range(2, 6):
        for i, where in ((0, ahead), (1, behind)):
            start(cot.at[:, half(CHUNK[g][i])], cm.at[g - 2, :, half(i)],
                  x_s.at[g - 2, i], x_r.at[g - 2, i], where)
    for g in range(2):
        start(cot.at[:, pl.ds(2 * g * ch, 2 * ch)], cp.at[g], c_s.at[g], c_r.at[g], partner)

    key_width = q1.shape[1] // 2
    value_width = val.shape[1] // 2
    block = tokens // 5

    def attend(h, out):
        ratio = mix[h]
        keyed = pl.ds(pl.multiple_of(h * key_width, key_width), key_width)
        valued = pl.ds(pl.multiple_of(h * value_width, value_width), value_width)
        for at in range(5):
            low, high = at * block, (at + 1) * block
            rows = lax.broadcasted_iota(jnp.int32, (block, high), 0) + low
            seen = lax.broadcasted_iota(jnp.int32, (block, high), 1) <= rows

            def probs(query, keys):
                scores = dot(query[low:high, keyed], keys[0:high, keyed], NT) * key_width ** (-0.5)
                scores = jnp.where(seen, scores, -jnp.inf)
                grown = jnp.exp(scores - jnp.max(scores, axis=1, keepdims=True))
                return grown, 1.0 / jnp.sum(grown, axis=1, keepdims=True)

            one, one_scale = probs(q1, k1)
            two, two_scale = probs(q2, k2)
            mixed = (one * one_scale - ratio * (two * two_scale)).astype(jnp.bfloat16)
            head = dot(mixed, val[0:high, valued])
            square = jnp.mean(head * head, axis=1, keepdims=True)
            normed = head * lax.rsqrt(square + epsilon) * gain[...]
            out[:, low:high] = normed.T.astype(jnp.bfloat16)

    def take(g):
        for i in range(2):
            arrived(cm.at[g - 2, :, half(i)], x_s.at[g - 2, i], x_r.at[g - 2, i])
        if g < 4:
            for i, where in ((0, ahead), (1, behind)):
                start(cm.at[g - 2, :, half(i)], cm.at[g + 2, :, half(i)],
                      x_s.at[g + 2, i], x_r.at[g + 2, i], where)
        start(cm.at[g - 2], cp.at[g], c_s.at[g], c_r.at[g], partner)

    attend(other, at_send)
    start(at_send, at_part, a_s, a_r, partner)
    take(2)
    attend(c, at_own)
    take(3)
    arrived(at_part, a_s, a_r)

    parts = gsend.shape[2]

    def summed(g):
        for d in range(1, n):
            arrived(rs1.at[g, d], r1_s.at[g, d], r1_r.at[g, d])
        total = rs1[g, 0].astype(jnp.float32)
        for d in range(1, n):
            total = total + rs1[g, d].astype(jnp.float32)
        s1b[g] = total.astype(jnp.bfloat16)

    for g in range(GROUPS):
        if g >= 4:
            take(g)
        mine = cot[:, 2 * g * ch : 2 * (g + 1) * ch] if g < 2 else cm[g - 2]
        grad = dot(at_own[...], mine)
        arrived(cp.at[g], c_s.at[g], c_r.at[g])
        grad = grad + dot(at_part[...], cp[g])
        gsend[g] = grad.reshape(n, parts, 2 * ch).astype(jnp.bfloat16)
        rs1[g, 0] = gsend[g, a]
        for d in range(1, n):
            p = around(a + d, n)
            start(gsend.at[g, p], rs1.at[g, d], r1_s.at[g, d], r1_r.at[g, d], at_a(p))
        if g >= 2:
            summed(g - 2)
    for g in range(GROUPS - 2, GROUPS):
        summed(g)

    per = GROUPS // n
    for d in range(1, n):
        p = around(b + d, n)
        start(s1b.at[pl.ds(p * per, per)], rs2.at[d], r2_s.at[d], r2_r.at[d], at_b(p))
    total = s1b[pl.ds(b * per, per)].astype(jnp.float32)
    for d in range(1, n):
        arrived(rs2.at[d], r2_s.at[d], r2_r.at[d])
        total = total + rs2[d].astype(jnp.float32)
    gall[c, a, pl.ds(b * per, per)] = total.astype(jnp.bfloat16)

    def gather(buf, count, b_s, b_r, a_s, a_r, d_s, d_r):
        own = buf.at[c, a, pl.ds(b * count, count)]
        for d in range(1, n):
            start(own, own, b_s.at[d], b_r.at[d], at_b(around(b + d, n)))
        for d in range(1, n):
            arrived(buf.at[c, a, pl.ds(around(b - d, n) * count, count)], b_s.at[d], b_r.at[d])
        line = buf.at[c, a]
        for d in range(1, n):
            start(line, line, a_s.at[d], a_r.at[d], at_a(around(a + d, n)))
        start(line, line, d_s.at[0], d_r.at[0], partner)
        for d in range(1, n):
            line = buf.at[c, around(a - d, n)]
            arrived(line, a_s.at[d], a_r.at[d])
            start(line, line, d_s.at[d], d_r.at[d], partner)
        for d in range(n):
            arrived(buf.at[other, around(b - d, n)], d_s.at[d], d_r.at[d])

    gather(gall, per, gb_s, gb_r, ga_s, ga_r, gd_s, gd_r)

    sources = (x, x, None, None, None, None, around(x + 2, nx), around(x + 2, nx))
    sides = (around(x - 1, nx), around(x + 1, nx))
    left_done = jnp.zeros(momentum.shape, jnp.float32)
    for g in range(GROUPS):
        columns = []
        for i in range(2):
            source = sides[i] if sources[g] is None else sources[g]
            at = pl.multiple_of((source * 4 + CHUNK[g][i]) * ch, ch)
            columns.append(left[:, pl.ds(at, ch)])
        grown = gall[:, :, g].reshape(2 * value_width, 2 * ch)
        left_done = left_done + dot(jnp.concatenate(columns, axis=1), grown, NT)

    high = left_done.astype(jnp.bfloat16)
    rest = left_done - high.astype(jnp.float32)
    middle = rest.astype(jnp.bfloat16)
    low = (rest - middle.astype(jnp.float32)).astype(jnp.bfloat16)
    done = []
    for h in range(2):
        columns = slice(h * value_width, (h + 1) * value_width)
        root = right[columns, :]
        done.append(dot(high[:, columns], root) + (dot(middle[:, columns], root) + dot(low[:, columns], root)))
    preconditioned = jnp.concatenate(done, axis=1)
    fresh = momentum_decay * momentum[...] + (1.0 - momentum_decay) * preconditioned
    momentum_out[...] = fresh

    def exchanged(value, slots, send, recv, where, at, size):
        slots[0] = value
        for d in range(1, size):
            start(slots.at[0], slots.at[d], send.at[d], recv.at[d], where(around(at + d, size)))
        for d in range(1, size):
            arrived(slots.at[d], send.at[d], recv.at[d])
            value = value + slots[d]
        return value

    squares = jnp.broadcast_to(jnp.sum(fresh * fresh, keepdims=True), ssx.shape[1:])
    squares = exchanged(squares, ssx, sx_s, sx_r, at_x, x, nx)
    squares = exchanged(squares, ssb, sb_s, sb_r, at_b, b, n)
    squares = exchanged(squares, ssa, sa_s, sa_r, at_a, a, n)
    squares = exchanged(squares, ssd, sd_s, sd_r, lambda p: partner, c, 2)
    factor = clip_level * lax.rsqrt(squares[0:1, 0:1] / entries + epsilon)
    step = factor * fresh + weight_decay * weight[...]
    step_out[...] = step
    new = weight[...] - step_rate * step
    weight_out[...] = new
    wall[c, a, b] = new.astype(jnp.bfloat16)
    gather(wall, 1, wb_s, wb_r, wa_s, wa_r, wd_s, wd_r)

    def laid(i, carry):
        copy_out[i, :, 0] = wall[0, i]
        copy_out[:, i, 1] = wall[1, i]
        return carry

    lax.fori_loop(0, n, laid, 0)
    for copy in pending:
        copy.wait_send()


def local(
    query_one, key_one, query_two, key_two, values, mix_ratio, head_gain,
    cotangent, left_roots, right_roots, weight, momentum,
):
    n = lax.axis_size("fs_0")
    nx = lax.axis_size("tp")
    tokens, own_cols = cotangent.shape
    rows = weight.shape[0]
    width = values.shape[1] // 2
    parts = width // n
    pair = own_cols // 2
    bf16, f32 = jnp.bfloat16, jnp.float32
    dma = pltpu.SemaphoreType.DMA
    vmem = pl.BlockSpec(memory_space=pltpu.VMEM)
    smem = pl.BlockSpec(memory_space=pltpu.SMEM)
    tile = (8, 128)
    shapes = pltpu.VMEM
    scratch = [
        shapes((GROUPS - 2, tokens, pair), bf16),
        shapes((GROUPS, tokens, pair), bf16),
        shapes((width, tokens), bf16),
        shapes((width, tokens), bf16),
        shapes((width, tokens), bf16),
        shapes((GROUPS, n, parts, pair), bf16),
        shapes((GROUPS, n, parts, pair), bf16),
        shapes((GROUPS, parts, pair), bf16),
        shapes((n, GROUPS // n, parts, pair), bf16),
        shapes((2, n, GROUPS, parts, pair), bf16),
        shapes((2, n, n, rows, own_cols), bf16),
        shapes((nx, *tile), f32),
        shapes((n, *tile), f32),
        shapes((n, *tile), f32),
        shapes((2, *tile), f32),
    ]
    for shape in ((GROUPS - 2, 2), (GROUPS,), (), (GROUPS, n), (n,), (n,), (n,), (n,), (n,), (n,), (n,), (nx,), (n,), (n,), (2,)):
        scratch += [dma(shape) if shape else dma] * 2
    step, weight_new, momentum_new, copied = pl.pallas_call(
        functools.partial(kernel, float(weight.size * n * n * 2 * nx)),
        out_shape=(
            jax.ShapeDtypeStruct(weight.shape, f32),
            jax.ShapeDtypeStruct(weight.shape, f32),
            jax.ShapeDtypeStruct(weight.shape, f32),
            jax.ShapeDtypeStruct((n, n, 2, rows, own_cols), bf16),
        ),
        in_specs=[vmem] * 5 + [smem] + [vmem] * 6,
        out_specs=[vmem] * 4,
        scratch_shapes=scratch,
        compiler_params=pltpu.CompilerParams(
            collective_id=0, has_side_effects=True, vmem_limit_bytes=60 * 1024 * 1024
        ),
    )(
        query_one, key_one, query_two, key_two, values, mix_ratio, head_gain.reshape(1, -1),
        cotangent, left_roots, right_roots, weight, momentum,
    )
    return step, weight_new, momentum_new, copied.reshape(-1, own_cols)


def split_mesh(mesh):
    lines = int((mesh.shape["fs"] // 2) ** 0.5)
    return Mesh(mesh.devices.reshape(lines, lines, 2, mesh.shape["tp"]), (*FS, "tp"))


def solution(mesh):
    return jax.shard_map(
        local,
        mesh=split_mesh(mesh),
        in_specs=(
            P(FS, "tp"), P(FS, "tp"), P(FS, "tp"), P(FS, "tp"), P(FS, "tp"), P("tp"), P(),
            P(FS, "tp"), P(FS, None), P("tp", None), P(FS, "tp"), P(FS, "tp"),
        ),
        out_specs=(P(FS, "tp"), P(FS, "tp"), P(FS, "tp"), P(None, "tp")),
        check_vma=False,
    )
```

time: 290 us -> 129 us (0.44)
  blocking collectives: 122 us -> 0 us
  Pallas kernels: 0 us -> 121 us
  waiting for transfers between devices: 94.1 us -> 0 us
  starting transfers between devices: 31.2 us -> 0 us
  matrix products: 17.8 us -> 0 us
  other arithmetic: 11.2 us -> 0 us
  local copies, waits for them, and re-layouts: 11.7 us -> 7.17 us
    all_to_all x6 -> x0, blocking collectives: 122 us -> none  [the longest x4 66.1 us: from_everyone(): lax.all_to_all(jnp.broadcast_to(shard[None], (length, *shard.shape)), axi...]
    pallas_call x0 -> x1, Pallas kernels: none -> 121 us  [local(): pl.pallas_call(functools.partial(kernel, float(weight.size * n * n * 2 *...]
    ppermute x7 -> x0, waiting for transfers between devices: 87.2 us -> none  [from_partner(): return lax.ppermute(block, axis, route)]
    ppermute x7 -> x0, starting transfers between devices: 26.4 us -> none  [from_partner(): return lax.ppermute(block, axis, route)]
    dot_general x6 -> x0, matrix products: 17.8 us -> none  [the longest x1 7.65 us: local(): jnp.einsum('hqk,khd->qhd', mixed, values.reshape(tok_rows, local_heads, v...]
    all_to_all x1 -> x0, waiting for transfers between devices: 6.9 us -> none  [from_everyone(): lax.all_to_all(jnp.broadcast_to(shard[None], (length, *shard.shape)), axi...]
    unnamed x21 -> x4, local copies, waits for them, and re-layouts: 1.48 us -> 7.17 us
    convert_element_type x16 -> x0, other arithmetic: 5.17 us -> none  [the longest x1 2.31 us: local(): (head_out * lax.rsqrt(square + epsilon) * head_gain).astype(jnp.bfloat16)]
  transfers between devices with their start and end apart: 8 -> 0, of which waited for: 8 -> 0; matrix products, arithmetic and copies ran while one was open for 7% -> 0% of each run, Pallas kernels for 0% -> 0%
where the time goes in v1:
time: 129 us; the launch traced here: 128 us
  Pallas kernels  121 us (94%)
  local copies, waits for them, and re-layouts  7.17 us (6%)
    pallas_call x1, Pallas kernels, local(): pl.pallas_call(functools.partial(kernel, float(weight.size * n * n * 2 *...  121 us
    unnamed x4, local copies, waits for them, and re-layouts  7.17 us

profile of v1, /device:TPU:1, one launch (start us, length us, event | category | flops | bytes accessed | tf_op | source)
XLA Modules:
  0.0 128.5 jit_solution(15514265594577235104)
XLA Ops:
  0.6 120.7 %shard_map.147 = (f32[16,512]{1,0:T(8,128)}, f32[16,512]{1,0:T(8,128)}, f32[16,512]{1,0:T(8,128)}, bf16[8,8,2,16,512]{4,3,2,1,0:T(8,128)(2,1)}) custom-call(bf16[640,256]{1,0:T(8,128)(2,1)} %q1.1, bf16[640,256]{1,0:T(8,128)(2,1)} %k1.1, bf16[640,256]{1,0:T(8,128)(2,1)} %q2.1, bf16[640,256]{1,0:T(8,128)(2,1)} %k2.1, bf16[640,512]{1,0:T(8,128)(2,1)} %val.1, ...), custom_call_target="tpu_custom_call" | custom-call | tf_op jit(solution)/shard_map/pallas_call | solution.py:291
  121.3 1.4 %copy.20 = f32[16,512]{1,0:T(8,128)} copy(f32[16,512]{1,0:T(8,128)} %get-tuple-element.16) | data formatting | bytes 65536
  122.7 1.4 %copy.21 = f32[16,512]{1,0:T(8,128)} copy(f32[16,512]{1,0:T(8,128)} %get-tuple-element.17) | data formatting | bytes 65536
  124.0 1.4 %copy.22 = f32[16,512]{1,0:T(8,128)} copy(f32[16,512]{1,0:T(8,128)} %get-tuple-element.18) | data formatting | bytes 65536
  125.4 3.0 %copy.23 = bf16[2048,512]{1,0:T(8,128)(2,1)} copy(bf16[2048,512]{1,0:T(8,128)(2,1)} %bitcast.2) | data formatting | bytes 4194304

commit v2 on v1

v2 whole, which is shorter than its diff:
```python
import functools

import jax
import jax.numpy as jnp
from jax import lax
from jax.experimental import pallas as pl
from jax.experimental.pallas import tpu as pltpu
from jax.sharding import Mesh
from jax.sharding import PartitionSpec as P

FS = ("fs_0", "fs_1", "fs_2")
MESH_ID = pl.DeviceIdType.MESH

epsilon = 1e-06
momentum_decay = 0.8
clip_level = 0.5
weight_decay = 0.2
step_rate = 0.1

GROUPS = 8
CHUNK = ((0, 1), (2, 3), (0, 2), (1, 3), (2, 0), (3, 1), (0, 2), (1, 3))
NT = (((1,), (1,)), ((), ()))


def dot(left, right, dims=(((1,), (0,)), ((), ()))):
    return lax.dot_general(left, right, dims, preferred_element_type=jnp.float32)


def kernel(
    entries,
    q1_in, k1_in, q2_in, k2_in, val_in, mix_in, gain_in, cot_in, left_in, right_in, weight_in, momentum_in,
    grown_out, factor_out, copy_out,
    q1, k1, q2, k2, val, mix, gain, cot, right, load,
    cm, cp, at_own, at_send, at_part, gsend, rs1, s1b, rs2, gall, wall, mall, ssx, ssa, ssd,
    left, momentum, grown_line,
    x_s, x_r, c_s, c_r, a_s, a_r, r1_s, r1_r, r2_s, r2_r,
    gb_s, gb_r, ga_s, ga_r, gd_s, gd_r, ma_s, ma_r, md_s, md_r,
    wb_s, wb_r, wa_s, wa_r, wd_s, wd_r, lb_s, lb_r, pb_s, pb_r,
    sx_s, sx_r, sa_s, sa_r, sd_s, sd_r,
):
    z, y, c, x = (lax.axis_index(name) for name in (*FS, "tp"))
    n = rs2.shape[0]
    nx = ssx.shape[0]
    other = 1 - c
    a = z * other + y * c
    b = y * other + z * c

    def at_a(p):
        return (p * other + z * c, y * other + p * c, c, x)

    def at_b(p):
        return (z * other + p * c, p * other + y * c, c, x)

    def at_x(p):
        return (z, y, c, p)

    partner = (z, y, other, x)

    def remote(src, dst, send, recv, where):
        return pltpu.make_async_remote_copy(
            src_ref=src, dst_ref=dst, send_sem=send, recv_sem=recv,
            device_id=where, device_id_type=MESH_ID,
        )

    def start(*parts):
        remote(*parts).start()

    def arrived(dst, send, recv):
        remote(dst, dst, send, recv, partner).wait_recv()

    def sent(src, send, recv):
        remote(src, src, send, recv, partner).wait_send()

    def around(p, size):
        return lax.rem(p + size, size)

    loads = {}
    for i, (name, src, dst) in enumerate((
        ("cot", cot_in, cot), ("q1", q1_in, q1), ("k1", k1_in, k1), ("q2", q2_in, q2), ("k2", k2_in, k2),
        ("val", val_in, val), ("gain", gain_in, gain), ("mix", mix_in, mix), ("weight", weight_in, wall.at[c, a, b]),
        ("left", left_in, left.at[b]), ("right", right_in, right), ("momentum", momentum_in, momentum.at[b]),
    )):
        loads[name] = pltpu.make_async_copy(src, dst, load.at[i])
        loads[name].start()

    barrier = pltpu.get_barrier_semaphore()
    peers = [partner]
    for d in range(1, n):
        peers += [at_a(around(a + d, n)), at_b(around(b + d, n))]
    for d in range(1, nx):
        peers.append(at_x(around(x + d, nx)))
    for peer in peers:
        pl.semaphore_signal(barrier, inc=1, device_id=peer, device_id_type=MESH_ID)
    pl.semaphore_wait(barrier, len(peers))

    tokens = cot.shape[0]
    ch = cot.shape[1] // 4
    ahead = at_x(around(x + 1, nx))
    behind = at_x(around(x - 1, nx))

    def half(i):
        return pl.ds(i * ch, ch)

    loads["cot"].wait()
    for g in range(2, 6):
        for i, where in ((0, ahead), (1, behind)):
            start(cot.at[:, half(CHUNK[g][i])], cm.at[g - 2, :, half(i)], x_s, x_r.at[g - 2], where)
    for g in range(2):
        start(cot.at[:, pl.ds(2 * g * ch, 2 * ch)], cp.at[g], c_s, c_r.at[g], partner)
    for name, held, send, recv in (
        ("weight", wall.at[c, a, b], wb_s, wb_r), ("momentum", momentum.at[b], pb_s, pb_r), ("left", left.at[b], lb_s, lb_r),
    ):
        loads[name].wait()
        for d in range(1, n):
            start(held, held, send, recv, at_b(around(b + d, n)))

    for name in ("q1", "k1", "q2", "k2", "val", "gain", "mix"):
        loads[name].wait()
    key_width = q1.shape[1] // 2
    value_width = val.shape[1] // 2
    block = tokens // 5

    def attend(h, out):
        chosen = lax.broadcasted_iota(jnp.int32, (1, 2), 1) == h
        ratio = jnp.sum(jnp.where(chosen, mix[...], 0.0), axis=1, keepdims=True)
        keyed = pl.ds(pl.multiple_of(h * key_width, key_width), key_width)
        valued = pl.ds(pl.multiple_of(h * value_width, value_width), value_width)
        for at in range(5):
            low, high = at * block, (at + 1) * block
            rows = lax.broadcasted_iota(jnp.int32, (block, high), 0) + low
            seen = lax.broadcasted_iota(jnp.int32, (block, high), 1) <= rows

            def probs(query, keys):
                scores = dot(query[low:high, keyed], keys[0:high, keyed], NT) * key_width ** (-0.5)
                scores = jnp.where(seen, scores, -jnp.inf)
                grown = jnp.exp(scores - jnp.max(scores, axis=1, keepdims=True))
                return grown, 1.0 / jnp.sum(grown, axis=1, keepdims=True)

            one, one_scale = probs(q1, k1)
            two, two_scale = probs(q2, k2)
            mixed = (one * one_scale - ratio * (two * two_scale)).astype(jnp.bfloat16)
            head = dot(mixed, val[0:high, valued])
            square = jnp.mean(head * head, axis=1, keepdims=True)
            normed = head * lax.rsqrt(square + epsilon) * gain[...]
            out[:, low:high] = normed.T.astype(jnp.bfloat16)

    def take(g):
        arrived(cm.at[g - 2], x_s, x_r.at[g - 2])
        if g < 4:
            for i, where in ((0, ahead), (1, behind)):
                start(cm.at[g - 2, :, half(i)], cm.at[g + 2, :, half(i)], x_s, x_r.at[g + 2], where)
        start(cm.at[g - 2], cp.at[g], c_s, c_r.at[g], partner)

    up = n // 2
    steps = [(h, 1, h == up) for h in range(1, up + 1)] + [(h, -1, h == n - 1 - up) for h in range(1, n - up)]

    def line_of(index, home):
        h, way, _ = steps[index]
        return around(home - way * h, n)

    def weight_lines(h):
        for index, (hop, way, last) in enumerate(steps):
            if hop != h:
                continue
            line = wall.at[c, line_of(index, a)]
            arrived(line, wa_s, wa_r.at[index])
            if not last:
                start(line, line, wa_s, wa_r.at[index + 1], at_a(around(a + way, n)))
            start(line, line, wd_s, wd_r, partner)

    attend(other, at_send)
    start(at_send, at_part, a_s, a_r, partner)
    take(2)
    arrived(wall.at[c, a, pl.ds(0, n - 1)], wb_s, wb_r)
    line = wall.at[c, a]
    for index, (h, way, _) in enumerate(steps):
        if h == 1:
            start(line, line, wa_s, wa_r.at[index], at_a(around(a + way, n)))
    start(line, line, wd_s, wd_r, partner)
    attend(c, at_own)
    take(3)
    arrived(at_part, a_s, a_r)

    parts = gsend.shape[2]
    others = pl.ds(1, n - 1)

    def summed(g):
        arrived(rs1.at[g, others], r1_s, r1_r.at[g])
        total = rs1[g, 0].astype(jnp.float32)
        for d in range(1, n):
            total = total + rs1[g, d].astype(jnp.float32)
        s1b[g] = total.astype(jnp.bfloat16)

    for g in range(GROUPS):
        if g >= 4:
            take(g)
        mine = cot[:, 2 * g * ch : 2 * (g + 1) * ch] if g < 2 else cm[g - 2]
        grad = dot(at_own[...], mine)
        arrived(cp.at[g], c_s, c_r.at[g])
        grad = grad + dot(at_part[...], cp[g])
        gsend[g] = grad.reshape(n, parts, 2 * ch).astype(jnp.bfloat16)
        rs1[g, 0] = gsend[g, a]
        for d in range(1, n):
            p = around(a + d, n)
            start(gsend.at[g, p], rs1.at[g, d], r1_s, r1_r.at[g], at_a(p))
        if g == 5:
            weight_lines(1)
        if g >= 5:
            summed(g - 5)
    weight_lines(2)
    sent(cm, x_s, x_r.at[0])
    sent(cp, c_s, c_r.at[0])
    sent(at_send, a_s, a_r)
    for g in range(GROUPS - 5, GROUPS):
        summed(g)

    per = GROUPS // n
    for d in range(1, n):
        p = around(b + d, n)
        start(s1b.at[pl.ds(p * per, per)], rs2.at[d], r2_s, r2_r, at_b(p))
    sent(rs1.at[:, others], r1_s, r1_r.at[0])
    sent(wall.at[c, a, pl.ds(0, n - 1)], wb_s, wb_r)
    for held, send, recv in ((momentum, pb_s, pb_r), (left, lb_s, lb_r)):
        sent(held.at[pl.ds(0, n - 1)], send, recv)
        arrived(held.at[pl.ds(0, n - 1)], send, recv)
    loads["right"].wait()
    total = s1b[pl.ds(b * per, per)].astype(jnp.float32)
    arrived(rs2.at[others], r2_s, r2_r)
    for d in range(1, n):
        total = total + rs2[d].astype(jnp.float32)
    gall[c, a, pl.ds(b * per, per)] = total.astype(jnp.bfloat16)

    own = gall.at[c, a, pl.ds(b * per, per)]
    for d in range(1, n):
        start(own, own, gb_s, gb_r, at_b(around(b + d, n)))
    sent(rs2.at[others], r2_s, r2_r)
    arrived(gall.at[c, a, pl.ds(0, (n - 1) * per)], gb_s, gb_r)

    def ring(buf, a_s, a_r, d_s, d_r, extra):
        pieces = a_r.shape[1]
        count = buf.shape[2] // pieces
        waiting = [pieces] * len(steps)

        def piece(line, k):
            return buf.at[c, line, pl.ds(k * count, count)]

        def step(index, k):
            _, way, last = steps[index]
            line = line_of(index, a)
            arrived(piece(line, k), a_s, a_r.at[index, k])
            if not last:
                start(piece(line, k), piece(line, k), a_s, a_r.at[index + 1, k], at_a(around(a + way, n)))
            waiting[index] -= 1
            if waiting[index] == 0:
                start(buf.at[c, line], buf.at[c, line], d_s, d_r, partner)

        for k in range(pieces):
            for index, (h, way, _) in enumerate(steps):
                if h == 1:
                    start(piece(a, k), piece(a, k), a_s, a_r.at[index, k], at_a(around(a + way, n)))
        start(buf.at[c, a], buf.at[c, a], d_s, d_r, partner)
        events = list(extra)
        for index, (h, _, _) in enumerate(steps):
            for k in range(pieces):
                events.append((2.05 * h + 0.35 * k, functools.partial(step, index, k)))
        for order, (_, event) in enumerate(sorted(events, key=lambda pair: pair[0])):
            event()

    def drained(buf, a_s, a_r, d_s, d_r):
        sent(buf.at[c, pl.ds(0, n - 1)], a_s, a_r)
        sent(buf.at[c], d_s, d_r)

    ring(gall, ga_s, ga_r, gd_s, gd_r, ())
    sent(gall.at[c, a, pl.ds(0, (n - 1) * per)], gb_s, gb_r)
    arrived(gall.at[other], gd_s, gd_r)
    weight_lines(3)

    sources = (x, x, None, None, None, None, around(x + 2, nx), around(x + 2, nx))
    sides = (around(x - 1, nx), around(x + 1, nx))
    rows = left.shape[1]
    left_done = jnp.zeros((n * rows, 2 * value_width), jnp.float32)
    for g in range(GROUPS):
        columns = []
        for i in range(2):
            source = sides[i] if sources[g] is None else sources[g]
            at = pl.multiple_of((source * 4 + CHUNK[g][i]) * ch, ch)
            columns.append(left[:, :, pl.ds(at, ch)].reshape(n * rows, ch))
        grown = gall[:, :, g].reshape(2 * value_width, 2 * ch)
        left_done = left_done + dot(jnp.concatenate(columns, axis=1), grown, NT)

    high = left_done.astype(jnp.bfloat16)
    rest = left_done - high.astype(jnp.float32)
    middle = rest.astype(jnp.bfloat16)
    low = (rest - middle.astype(jnp.float32)).astype(jnp.bfloat16)
    done = []
    for h in range(2):
        columns = slice(h * value_width, (h + 1) * value_width)
        root = right[columns, :]
        done.append(dot(high[:, columns], root) + (dot(middle[:, columns], root) + dot(low[:, columns], root)))
    preconditioned = jnp.concatenate(done, axis=1)
    grown_line[...] = preconditioned.reshape(grown_line.shape)
    fresh = momentum_decay * momentum[...] + (1.0 - momentum_decay) * preconditioned.reshape(grown_line.shape)
    mall[c, a] = fresh.astype(jnp.bfloat16)

    def offered(value, slots, send, recv, where, at, size):
        slots[at] = value
        for d in range(1, size):
            start(slots.at[at], slots.at[at], send, recv, where(around(at + d, size)))

    stages = (
        (ssx, sx_s, sx_r, at_x, x, nx), (ssa, sa_s, sa_r, at_a, a, n), (ssd, sd_s, sd_r, lambda p: partner, c, 2),
    )
    squares = jnp.sum(jnp.sum(fresh * fresh, axis=0), keepdims=True)
    offered(jnp.broadcast_to(squares, ssx.shape[1:]), *stages[0])
    total = []

    def pass_on(index):
        slots, send, recv, _, _, size = stages[index]
        arrived(slots.at[pl.ds(0, size - 1)], send, recv)
        squares = jnp.sum(slots[...], axis=0)
        if index + 1 < len(stages):
            offered(squares, *stages[index + 1])
        else:
            total.append(squares)

    ring(mall, ma_s, ma_r, md_s, md_r,
         [(when, functools.partial(pass_on, index)) for index, when in enumerate((2.8, 7.3, 8.3))])
    factor = clip_level * lax.rsqrt(total[0] / entries + epsilon)
    factor_out[...] = factor
    grown_out[...] = grown_line[b]
    weight_lines(4)
    arrived(wall.at[other], wd_s, wd_r)
    scale = factor[0:1, 0:1].reshape(1, 1, 1)

    def final(core, line):
        held = wall[core, line]
        step = scale * mall[core, line].astype(jnp.float32) + weight_decay * held
        return (held - step_rate * step).astype(jnp.bfloat16)

    arrived(mall.at[other], md_s, md_r)

    def laid(i, carry):
        copy_out[i, :, 0] = final(0, i)
        copy_out[:, i, 1] = final(1, i)
        return carry

    lax.fori_loop(0, n, laid, 0)
    drained(gall, ga_s, ga_r.at[0, 0], gd_s, gd_r)
    drained(mall, ma_s, ma_r.at[0, 0], md_s, md_r)
    drained(wall, wa_s, wa_r.at[0], wd_s, wd_r)
    for slots, send, recv, _, _, size in stages:
        sent(slots.at[pl.ds(0, size - 1)], send, recv)


def local(
    query_one, key_one, query_two, key_two, values, mix_ratio, head_gain,
    cotangent, left_roots, right_roots, weight, momentum,
):
    n = lax.axis_size("fs_0")
    nx = lax.axis_size("tp")
    tokens, own_cols = cotangent.shape
    rows = weight.shape[0]
    width = values.shape[1] // 2
    parts = width // n
    pair = own_cols // 2
    bf16, f32 = jnp.bfloat16, jnp.float32
    dma = pltpu.SemaphoreType.DMA
    vmem = pl.BlockSpec(memory_space=pltpu.VMEM)
    hbm = pl.BlockSpec(memory_space=pltpu.HBM)
    tile = (8, 128)
    shapes = pltpu.VMEM
    gain, mix = head_gain.reshape(1, -1), mix_ratio.reshape(1, -1)
    scratch = [
        shapes(array.shape, array.dtype)
        for array in (query_one, key_one, query_two, key_two, values, mix, gain, cotangent, right_roots)
    ]
    scratch += [
        dma((12,)),
        shapes((GROUPS - 2, tokens, pair), bf16),
        shapes((GROUPS, tokens, pair), bf16),
        shapes((width, tokens), bf16),
        shapes((width, tokens), bf16),
        shapes((width, tokens), bf16),
        shapes((GROUPS, n, parts, pair), bf16),
        shapes((GROUPS, n, parts, pair), bf16),
        shapes((GROUPS, parts, pair), bf16),
        shapes((n, GROUPS // n, parts, pair), bf16),
        shapes((2, n, GROUPS, parts, pair), bf16),
        shapes((2, n, n, rows, own_cols), f32),
        shapes((2, n, n, rows, own_cols), bf16),
        shapes((nx, *tile), f32),
        shapes((n, *tile), f32),
        shapes((2, *tile), f32),
        shapes((n, *left_roots.shape), bf16),
        shapes((n, rows, own_cols), f32),
        shapes((n, rows, own_cols), f32),
    ]
    pieces = min(4, n)
    for received in (
        (GROUPS - 2,), (GROUPS,), (), (GROUPS,), (), (), (n - 1, pieces), (), (n - 1, pieces), (),
        (), (n - 1,), (), (), (), (), (), (),
    ):
        scratch += [dma, dma(received) if received else dma]
    inputs = [
        pltpu.with_memory_space_constraint(array, pltpu.HBM)
        for array in (
            query_one, key_one, query_two, key_two, values, mix, gain,
            cotangent, left_roots, right_roots, weight, momentum,
        )
    ]
    grown, factor, copied = pl.pallas_call(
        functools.partial(kernel, float(weight.size * n * n * 2 * nx)),
        out_shape=(
            jax.ShapeDtypeStruct(weight.shape, f32),
            jax.ShapeDtypeStruct(tile, f32),
            jax.ShapeDtypeStruct((n, n, 2, rows, own_cols), bf16),
        ),
        in_specs=[hbm] * 12,
        out_specs=[vmem] * 3,
        scratch_shapes=scratch,
        compiler_params=pltpu.CompilerParams(
            collective_id=0, has_side_effects=True, vmem_limit_bytes=40 * 1024 * 1024
        ),
    )(*inputs)
    momentum_new = momentum_decay * momentum + (1.0 - momentum_decay) * grown
    step = factor[0, 0] * momentum_new + weight_decay * weight
    weight_new = weight - step_rate * step
    return step, weight_new, momentum_new, copied.reshape(-1, own_cols)


def split_mesh(mesh):
    lines = int((mesh.shape["fs"] // 2) ** 0.5)
    return Mesh(mesh.devices.reshape(lines, lines, 2, mesh.shape["tp"]), (*FS, "tp"))


def solution(mesh):
    return jax.shard_map(
        local,
        mesh=split_mesh(mesh),
        in_specs=(
            P(FS, "tp"), P(FS, "tp"), P(FS, "tp"), P(FS, "tp"), P(FS, "tp"), P("tp"), P(),
            P(FS, "tp"), P(FS, None), P("tp", None), P(FS, "tp"), P(FS, "tp"),
        ),
        out_specs=(P(FS, "tp"), P(FS, "tp"), P(FS, "tp"), P(None, "tp")),
        check_vma=False,
    )
```

time: 129 us -> 96.5 us (0.75)
  Pallas kernels: 121 us -> 92.5 us
  local copies, waits for them, and re-layouts: 7.17 us -> 1.84 us
  other arithmetic: 0 us -> 1.29 us
    pallas_call x1, Pallas kernels: 121 us -> 92.5 us  [local(): pl.pallas_call(functools.partial(kernel, float(weight.size * n * n * 2 *...]
    unnamed x4 -> x5, local copies, waits for them, and re-layouts: 7.17 us -> 1.33 us
    sub x0 -> x1, other arithmetic: none -> 1.29 us  [local(): weight_new = weight - step_rate * step]
where the time goes in v2:
time: 96.5 us; the launch traced here: 96.3 us
  Pallas kernels  92.5 us (96%)
  local copies, waits for them, and re-layouts  1.84 us (2%)
  other arithmetic  1.29 us (1%)
    pallas_call x1, Pallas kernels, local(): pl.pallas_call(functools.partial(kernel, float(weight.size * n * n * 2 *...  92.5 us

profile of v2, /device:TPU:1, one launch (start us, length us, event | category | flops | bytes accessed | tf_op | source)
XLA Modules:
  0.0 96.3 jit_solution(12954256671681018121)
XLA Ops:
  0.6 0.0 copy-start.1
  0.6 0.0 copy-start
  0.7 92.5 %shard_map.147 = (f32[16,512]{1,0:T(8,128)S(1)}, f32[8,128]{1,0:T(8,128)S(1)}, bf16[8,8,2,16,512]{4,3,2,1,0:T(8,128)(2,1)S(1)}) custom-call(bf16[640,256]{1,0:T(8,128)(2,1)} %q1_in.1, bf16[640,256]{1,0:T(8,128)(2,1)} %k1_in.1, bf16[640,256]{1,0:T(8,128)(2,1)} %q2_in.1, bf16[640,256]{1,0:T(8,128)(2,1)} %k2_in.1, bf16[640,512]{1,0:T(8,128)(2,1)} %val_in.1, ...), custom_call_target="tpu_custom_call" | custom-call | tf_op jit(solution)/shard_map/pallas_call | solution.py:411
  93.2 0.5 slice.3
  93.7 0.0 copy-done.1
  93.7 0.0 copy-done
  93.7 1.3 %multiply_subtract_fusion = (f32[16,512]{1,0:T(8,128)}, f32[16,512]{1,0:T(8,128)}, f32[16,512]{1,0:T(8,128)}) fusion(f32[16,512]{1,0:T(8,128)S(1)} %copy-done, f32[]{:T(128)} %bitcast.2, f32[16,512]{1,0:T(8,128)S(1)} %get-tuple-element.8, f32[16,512]{1,0:T(8,128)S(1)} %copy-done.1), kind=kLoop, calls=%fused_computation | loop fusion | flops 65536 | bytes 196612 | tf_op jit(solution)/shard_map/sub | solution.py:427
  95.0 1.3 %copy.17 = bf16[2048,512]{1,0:T(8,128)(2,1)} copy(bf16[2048,512]{1,0:T(8,128)(2,1)S(1)} %bitcast.4) | data formatting | bytes 4194304
Async XLA Ops:
  0.6 93.1 %copy-start.1 = (f32[16,512]{1,0:T(8,128)S(1)}, f32[16,512]{1,0:T(8,128)}, u32[]{:S(2)}) copy-start(f32[16,512]{1,0:T(8,128)} %momentum_in.1) | copy-start | bytes 98308
  0.6 93.1 %copy-start = (f32[16,512]{1,0:T(8,128)S(1)}, f32[16,512]{1,0:T(8,128)}, u32[]{:S(2)}) copy-start(f32[16,512]{1,0:T(8,128)} %weight_in.1) | copy-start | bytes 98308

commit v3 on v2

--- a/solution.py
+++ b/solution.py
@@ -203,11 +203,9 @@
         for d in range(1, n):
             p = around(a + d, n)
             start(gsend.at[g, p], rs1.at[g, d], r1_s, r1_r.at[g], at_a(p))
-        if g == 5:
-            weight_lines(1)
         if g >= 5:
             summed(g - 5)
-    weight_lines(2)
+    weight_lines(1)
     sent(cm, x_s, x_r.at[0])
     sent(cp, c_s, c_r.at[0])
     sent(at_send, a_s, a_r)
@@ -219,6 +217,7 @@
         p = around(b + d, n)
         start(s1b.at[pl.ds(p * per, per)], rs2.at[d], r2_s, r2_r, at_b(p))
     sent(rs1.at[:, others], r1_s, r1_r.at[0])
+    weight_lines(2)
     sent(wall.at[c, a, pl.ds(0, n - 1)], wb_s, wb_r)
     for held, send, recv in ((momentum, pb_s, pb_r), (left, lb_s, lb_r)):
         sent(held.at[pl.ds(0, n - 1)], send, recv)
@@ -234,35 +233,50 @@
     for d in range(1, n):
         start(own, own, gb_s, gb_r, at_b(around(b + d, n)))
     sent(rs2.at[others], r2_s, r2_r)
+    weight_lines(3)
     arrived(gall.at[c, a, pl.ds(0, (n - 1) * per)], gb_s, gb_r)
 
-    def ring(buf, a_s, a_r, d_s, d_r, extra):
+    down = n - 1 - up
+    away = list(range(1, up + 1)) + [-d for d in range(1, down + 1)]
+
+    def spread(buf, a_s, a_r, d_s, d_r, extra):
         pieces = a_r.shape[1]
         count = buf.shape[2] // pieces
-        waiting = [pieces] * len(steps)
-
-        def piece(line, k):
-            return buf.at[c, line, pl.ds(k * count, count)]
-
-        def step(index, k):
-            _, way, last = steps[index]
-            line = line_of(index, a)
-            arrived(piece(line, k), a_s, a_r.at[index, k])
-            if not last:
-                start(piece(line, k), piece(line, k), a_s, a_r.at[index + 1, k], at_a(around(a + way, n)))
+        waiting = [pieces] * len(away)
+
+        def send(line, k, to, index):
+            part = buf.at[c, line, pl.ds(k * count, count)]
+            start(part, part, a_s, a_r.at[index, k], at_a(around(a + to, n)))
+
+        def step(s, k):
+            index = away.index(s)
+            line = around(a - s, n)
+            arrived(buf.at[c, line, pl.ds(k * count, count)], a_s, a_r.at[index, k])
+            if s == 2:
+                if up > 3 and k % 2 == 0:
+                    send(line, k, 2, away.index(4))
+                if up > 2:
+                    send(line, k, 1, away.index(3))
+            if s == -2:
+                if up > 3 and k % 2 == 1:
+                    send(line, k, -2, away.index(4))
+                if down > 2:
+                    send(line, k, -1, away.index(-3))
             waiting[index] -= 1
             if waiting[index] == 0:
                 start(buf.at[c, line], buf.at[c, line], d_s, d_r, partner)
 
-        for k in range(pieces):
-            for index, (h, way, _) in enumerate(steps):
-                if h == 1:
-                    start(piece(a, k), piece(a, k), a_s, a_r.at[index, k], at_a(around(a + way, n)))
+        for near in (2, 1):
+            for k in range(pieces):
+                for s in (near, -near):
+                    if s in away:
+                        send(a, k, s, away.index(s))
         start(buf.at[c, a], buf.at[c, a], d_s, d_r, partner)
         events = list(extra)
-        for index, (h, _, _) in enumerate(steps):
+        late = {1: 5.0, 2: 3.4, 3: 6.4, 4: 7.4}
+        for s in away:
             for k in range(pieces):
-                events.append((2.05 * h + 0.35 * k, functools.partial(step, index, k)))
+                events.append((late[abs(s)] + 0.5 * k, functools.partial(step, s, k)))
         for order, (_, event) in enumerate(sorted(events, key=lambda pair: pair[0])):
             event()
 
@@ -270,10 +284,9 @@
         sent(buf.at[c, pl.ds(0, n - 1)], a_s, a_r)
         sent(buf.at[c], d_s, d_r)
 
-    ring(gall, ga_s, ga_r, gd_s, gd_r, ())
+    spread(gall, ga_s, ga_r, gd_s, gd_r, ())
     sent(gall.at[c, a, pl.ds(0, (n - 1) * per)], gb_s, gb_r)
     arrived(gall.at[other], gd_s, gd_r)
-    weight_lines(3)
 
     sources = (x, x, None, None, None, None, around(x + 2, nx), around(x + 2, nx))
     sides = (around(x - 1, nx), around(x + 1, nx))
@@ -323,10 +336,10 @@
         else:
             total.append(squares)
 
-    ring(mall, ma_s, ma_r, md_s, md_r,
-         [(when, functools.partial(pass_on, index)) for index, when in enumerate((2.8, 7.3, 8.3))])
+    spread(mall, ma_s, ma_r, md_s, md_r,
+           [(when, functools.partial(pass_on, index)) for index, when in enumerate((2.8, 6.6, 9.3))])
     factor = clip_level * lax.rsqrt(total[0] / entries + epsilon)
-    factor_out[...] = factor
+    factor_out[...] = jnp.broadcast_to(factor[0:1, 0:1], factor_out.shape)
     grown_out[...] = grown_line[b]
     weight_lines(4)
     arrived(wall.at[other], wd_s, wd_r)
@@ -412,7 +425,7 @@
         functools.partial(kernel, float(weight.size * n * n * 2 * nx)),
         out_shape=(
             jax.ShapeDtypeStruct(weight.shape, f32),
-            jax.ShapeDtypeStruct(tile, f32),
+            jax.ShapeDtypeStruct(weight.shape, f32),
             jax.ShapeDtypeStruct((n, n, 2, rows, own_cols), bf16),
         ),
         in_specs=[hbm] * 12,
@@ -423,7 +436,7 @@
         ),
     )(*inputs)
     momentum_new = momentum_decay * momentum + (1.0 - momentum_decay) * grown
-    step = factor[0, 0] * momentum_new + weight_decay * weight
+    step = factor * momentum_new + weight_decay * weight
     weight_new = weight - step_rate * step
     return step, weight_new, momentum_new, copied.reshape(-1, own_cols)
 

time: 96.5 us -> 89.1 us (0.923)
  Pallas kernels: 92.5 us -> 86.3 us
    pallas_call x1, Pallas kernels: 92.5 us -> 86.3 us  [local(): pl.pallas_call(functools.partial(kernel, float(weight.size * n * n * 2 *...]
where the time goes in v3:
time: 89.1 us; the launch traced here: 88.9 us
  Pallas kernels  86.3 us (97%)
  local copies, waits for them, and re-layouts  1.33 us (1%)
    pallas_call x1, Pallas kernels, local(): pl.pallas_call(functools.partial(kernel, float(weight.size * n * n * 2 *...  86.3 us

profile of v3, /device:TPU:1, one launch (start us, length us, event | category | flops | bytes accessed | tf_op | source)
XLA Modules:
  0.0 88.9 jit_solution(8806036444266960968)
XLA Ops:
  0.6 0.0 copy-start.1
  0.6 0.0 copy-start
  0.7 86.3 %shard_map.147 = (f32[16,512]{1,0:T(8,128)S(1)}, f32[16,512]{1,0:T(8,128)S(1)}, bf16[8,8,2,16,512]{4,3,2,1,0:T(8,128)(2,1)S(1)}) custom-call(bf16[640,256]{1,0:T(8,128)(2,1)} %q1_in.1, bf16[640,256]{1,0:T(8,128)(2,1)} %k1_in.1, bf16[640,256]{1,0:T(8,128)(2,1)} %q2_in.1, bf16[640,256]{1,0:T(8,128)(2,1)} %k2_in.1, bf16[640,512]{1,0:T(8,128)(2,1)} %val_in.1, ...), custom_call_target="tpu_custom_call" | custom-call | tf_op jit(solution)/shard_map/pallas_call | solution.py:424
  86.9 0.0 copy-done.1
  86.9 0.0 copy-done
  87.0 0.6 multiply_subtract_fusion
  87.6 1.3 %copy.17 = bf16[2048,512]{1,0:T(8,128)(2,1)} copy(bf16[2048,512]{1,0:T(8,128)(2,1)S(1)} %bitcast.3) | data formatting | bytes 4194304
Async XLA Ops:
  0.6 86.3 %copy-start.1 = (f32[16,512]{1,0:T(8,128)S(1)}, f32[16,512]{1,0:T(8,128)}, u32[]{:S(2)}) copy-start(f32[16,512]{1,0:T(8,128)} %momentum_in.1) | copy-start | bytes 98308
  0.6 86.3 %copy-start = (f32[16,512]{1,0:T(8,128)S(1)}, f32[16,512]{1,0:T(8,128)}, u32[]{:S(2)}) copy-start(f32[16,512]{1,0:T(8,128)} %weight_in.1) | copy-start | bytes 98308

commit v4 on v3

--- a/solution.py
+++ b/solution.py
@@ -18,6 +18,7 @@
 step_rate = 0.1
 
 GROUPS = 8
+LAST = 3
 CHUNK = ((0, 1), (2, 3), (0, 2), (1, 3), (2, 0), (3, 1), (0, 2), (1, 3))
 NT = (((1,), (1,)), ((), ()))
 
@@ -31,11 +32,11 @@
     q1_in, k1_in, q2_in, k2_in, val_in, mix_in, gain_in, cot_in, left_in, right_in, weight_in, momentum_in,
     grown_out, factor_out, copy_out,
     q1, k1, q2, k2, val, mix, gain, cot, right, load,
-    cm, cp, at_own, at_send, at_part, gsend, rs1, s1b, rs2, gall, wall, mall, ssx, ssa, ssd,
+    cm, cp, at_own, at_send, at_part, gsend, rs1, s1b, rs2, rsb, gall, wall, mall, ssx, ssa, ssd,
     left, momentum, grown_line,
-    x_s, x_r, c_s, c_r, a_s, a_r, r1_s, r1_r, r2_s, r2_r,
+    x_s, x_r, c_s, c_r, a_s, a_r, r1_s, r1_r, r2_s, r2_r, rb_s, rb_r,
     gb_s, gb_r, ga_s, ga_r, gd_s, gd_r, ma_s, ma_r, md_s, md_r,
-    wb_s, wb_r, wa_s, wa_r, wd_s, wd_r, lb_s, lb_r, pb_s, pb_r,
+    wb_s, wb_r, wa_s, wa_r, wd_s, wd_r, lb_s, lb_r, lx_s, lx_r, pb_s, pb_r,
     sx_s, sx_r, sa_s, sa_r, sd_s, sd_r,
 ):
     z, y, c, x = (lax.axis_index(name) for name in (*FS, "tp"))
@@ -78,7 +79,7 @@
     for i, (name, src, dst) in enumerate((
         ("cot", cot_in, cot), ("q1", q1_in, q1), ("k1", k1_in, k1), ("q2", q2_in, q2), ("k2", k2_in, k2),
         ("val", val_in, val), ("gain", gain_in, gain), ("mix", mix_in, mix), ("weight", weight_in, wall.at[c, a, b]),
-        ("left", left_in, left.at[b]), ("right", right_in, right), ("momentum", momentum_in, momentum.at[b]),
+        ("left", left_in.at[:, pl.ds(pl.multiple_of(x * cot.shape[1], cot.shape[1]), cot.shape[1])], left.at[0, b]), ("right", right_in, right), ("momentum", momentum_in, momentum.at[b]),
     )):
         loads[name] = pltpu.make_async_copy(src, dst, load.at[i])
         loads[name].start()
@@ -107,12 +108,18 @@
             start(cot.at[:, half(CHUNK[g][i])], cm.at[g - 2, :, half(i)], x_s, x_r.at[g - 2], where)
     for g in range(2):
         start(cot.at[:, pl.ds(2 * g * ch, 2 * ch)], cp.at[g], c_s, c_r.at[g], partner)
+    up = n // 2
+    down = n - 1 - up
+    away = list(range(1, up + 1)) + [-d for d in range(1, down + 1)]
     for name, held, send, recv in (
-        ("weight", wall.at[c, a, b], wb_s, wb_r), ("momentum", momentum.at[b], pb_s, pb_r), ("left", left.at[b], lb_s, lb_r),
+        ("weight", wall.at[c, a, b], wb_s, wb_r), ("momentum", momentum.at[b], pb_s, pb_r),
     ):
         loads[name].wait()
         for d in range(1, n):
             start(held, held, send, recv, at_b(around(b + d, n)))
+    loads["left"].wait()
+    for d in range(1, n):
+        start(left.at[0, b], left.at[0, b], lb_s, lb_r, at_b(around(b + d, n)))
 
     for name in ("q1", "k1", "q2", "k2", "val", "gain", "mix"):
         loads[name].wait()
@@ -151,7 +158,6 @@
                 start(cm.at[g - 2, :, half(i)], cm.at[g + 2, :, half(i)], x_s, x_r.at[g + 2], where)
         start(cm.at[g - 2], cp.at[g], c_s, c_r.at[g], partner)
 
-    up = n // 2
     steps = [(h, 1, h == up) for h in range(1, up + 1)] + [(h, -1, h == n - 1 - up) for h in range(1, n - up)]
 
     def line_of(index, home):
@@ -170,15 +176,7 @@
 
     attend(other, at_send)
     start(at_send, at_part, a_s, a_r, partner)
-    take(2)
-    arrived(wall.at[c, a, pl.ds(0, n - 1)], wb_s, wb_r)
-    line = wall.at[c, a]
-    for index, (h, way, _) in enumerate(steps):
-        if h == 1:
-            start(line, line, wa_s, wa_r.at[index], at_a(around(a + way, n)))
-    start(line, line, wd_s, wd_r, partner)
     attend(c, at_own)
-    take(3)
     arrived(at_part, a_s, a_r)
 
     parts = gsend.shape[2]
@@ -191,9 +189,60 @@
             total = total + rs1[g, d].astype(jnp.float32)
         s1b[g] = total.astype(jnp.bfloat16)
 
+    per = GROUPS // n
+
+    early = GROUPS - LAST
+
+    def owned(p):
+        return len([g for g in range(early) if g // per == p])
+
+    def finish(g):
+        summed(g)
+        if g >= early:
+            rsb[g - early, b] = s1b[g]
+            for d in range(1, n):
+                start(s1b.at[g], rsb.at[g - early, b], rb_s, rb_r.at[g - early], at_b(around(b + d, n)))
+            return
+        owner = g // per
+
+        @pl.when(b != owner)
+        def _():
+            start(s1b.at[g], rs2.at[around(b - owner, n), g % per], r2_s, r2_r.at[g % per], at_b(owner))
+
+    def own(g):
+        @pl.when(b == g // per)
+        def _():
+            arrived(rs2.at[others, g % per], r2_s, r2_r.at[g % per])
+            total = s1b[g].astype(jnp.float32)
+            for d in range(1, n):
+                total = total + rs2[d, g % per].astype(jnp.float32)
+            gall[c, a, g] = total.astype(jnp.bfloat16)
+            for d in range(1, n):
+                start(gall.at[c, a, g], gall.at[c, a, g], gb_s, gb_r.at[g], at_b(around(b + d, n)))
+
+    def whole(g):
+        if g >= early:
+            arrived(rsb.at[g - early, others], rb_s, rb_r.at[g - early])
+            total = rsb[g - early, 0].astype(jnp.float32)
+            for p in range(1, n):
+                total = total + rsb[g - early, p].astype(jnp.float32)
+            gall[c, a, g] = total.astype(jnp.bfloat16)
+            return
+
+        @pl.when(b != g // per)
+        def _():
+            arrived(gall.at[c, a, g], gb_s, gb_r.at[g])
+
     for g in range(GROUPS):
-        if g >= 4:
+        if g >= 2:
             take(g)
+        if g == 2:
+            arrived(wall.at[c, a, pl.ds(0, n - 1)], wb_s, wb_r)
+            line = wall.at[c, a]
+            for index, (h, way, _) in enumerate(steps):
+                if h == 1:
+                    start(line, line, wa_s, wa_r.at[index], at_a(around(a + way, n)))
+            start(line, line, wd_s, wd_r, partner)
         mine = cot[:, 2 * g * ch : 2 * (g + 1) * ch] if g < 2 else cm[g - 2]
         grad = dot(at_own[...], mine)
         arrived(cp.at[g], c_s, c_r.at[g])
@@ -203,50 +252,54 @@
         for d in range(1, n):
             p = around(a + d, n)
             start(gsend.at[g, p], rs1.at[g, d], r1_s, r1_r.at[g], at_a(p))
+        if g == 5:
+            weight_lines(1)
         if g >= 5:
-            summed(g - 5)
-    weight_lines(1)
+            finish(g - 5)
+    arrived(left.at[0, pl.ds(0, n - 1)], lb_s, lb_r)
+    for d in range(1, nx):
+        start(left.at[0], left.at[d], lx_s, lx_r, at_x(around(x + d, nx)))
     sent(cm, x_s, x_r.at[0])
     sent(cp, c_s, c_r.at[0])
     sent(at_send, a_s, a_r)
-    for g in range(GROUPS - 5, GROUPS):
-        summed(g)
-
-    per = GROUPS // n
-    for d in range(1, n):
-        p = around(b + d, n)
-        start(s1b.at[pl.ds(p * per, per)], rs2.at[d], r2_s, r2_r, at_b(p))
-    sent(rs1.at[:, others], r1_s, r1_r.at[0])
+    sent(wall.at[c, a, pl.ds(0, n - 1)], wb_s, wb_r)
+    sent(momentum.at[pl.ds(0, n - 1)], pb_s, pb_r)
+    arrived(momentum.at[pl.ds(0, n - 1)], pb_s, pb_r)
+    sent(left.at[0, pl.ds(0, n - 1)], lb_s, lb_r)
+    loads["right"].wait()
+    finish(3)
+    finish(4)
+    own(0)
+    own(1)
+    own(2)
+    finish(5)
+    own(3)
+    finish(6)
+    own(4)
+    finish(7)
+
     weight_lines(2)
-    sent(wall.at[c, a, pl.ds(0, n - 1)], wb_s, wb_r)
-    for held, send, recv in ((momentum, pb_s, pb_r), (left, lb_s, lb_r)):
-        sent(held.at[pl.ds(0, n - 1)], send, recv)
-        arrived(held.at[pl.ds(0, n - 1)], send, recv)
-    loads["right"].wait()
-    total = s1b[pl.ds(b * per, per)].astype(jnp.float32)
-    arrived(rs2.at[others], r2_s, r2_r)
-    for d in range(1, n):
-        total = total + rs2[d].astype(jnp.float32)
-    gall[c, a, pl.ds(b * per, per)] = total.astype(jnp.bfloat16)
-
-    own = gall.at[c, a, pl.ds(b * per, per)]
-    for d in range(1, n):
-        start(own, own, gb_s, gb_r, at_b(around(b + d, n)))
-    sent(rs2.at[others], r2_s, r2_r)
-    weight_lines(3)
-    arrived(gall.at[c, a, pl.ds(0, (n - 1) * per)], gb_s, gb_r)
-
-    down = n - 1 - up
-    away = list(range(1, up + 1)) + [-d for d in range(1, down + 1)]
-
-    def spread(buf, a_s, a_r, d_s, d_r, extra):
+
+    def spread(buf, a_s, a_r, d_s, d_r, entries, extra):
         pieces = a_r.shape[1]
         count = buf.shape[2] // pieces
-        waiting = [pieces] * len(away)
+        waiting = [pieces] * (len(away) + 1)
+
+        def done(index, line):
+            waiting[index] -= 1
+            if waiting[index] == 0:
+                start(buf.at[c, line], buf.at[c, line], d_s, d_r, partner)
 
         def send(line, k, to, index):
             part = buf.at[c, line, pl.ds(k * count, count)]
             start(part, part, a_s, a_r.at[index, k], at_a(around(a + to, n)))
+
+        def enter(k, ready):
+            ready()
+            for s in (2, -2, 1, -1):
+                if s in away:
+                    send(a, k, s, away.index(s))
+            done(len(away), a)
 
         def step(s, k):
             index = away.index(s)
@@ -262,42 +315,52 @@
                     send(line, k, -2, away.index(4))
                 if down > 2:
                     send(line, k, -1, away.index(-3))
-            waiting[index] -= 1
-            if waiting[index] == 0:
-                start(buf.at[c, line], buf.at[c, line], d_s, d_r, partner)
-
-        for near in (2, 1):
-            for k in range(pieces):
-                for s in (near, -near):
-                    if s in away:
-                        send(a, k, s, away.index(s))
-        start(buf.at[c, a], buf.at[c, a], d_s, d_r, partner)
+            done(index, line)
+
         events = list(extra)
-        late = {1: 5.0, 2: 3.4, 3: 6.4, 4: 7.4}
-        for s in away:
-            for k in range(pieces):
-                events.append((late[abs(s)] + 0.5 * k, functools.partial(step, s, k)))
+        late = {1: 5.0, 2: 3.6, 3: 6.4, 4: 7.4}
+        for k in range(pieces):
+            when, ready = entries[k]
+            events.append((when, functools.partial(enter, k, ready)))
+            for s in away:
+                events.append((when + late[abs(s)], functools.partial(step, s, k)))
         for order, (_, event) in enumerate(sorted(events, key=lambda pair: pair[0])):
             event()
+
+    pieces = ga_r.shape[1]
+    count = GROUPS // pieces
+
+    def whole_piece(k):
+        for g in range(k * count, (k + 1) * count):
+            whole(g)
 
     def drained(buf, a_s, a_r, d_s, d_r):
         sent(buf.at[c, pl.ds(0, n - 1)], a_s, a_r)
         sent(buf.at[c], d_s, d_r)
 
-    spread(gall, ga_s, ga_r, gd_s, gd_r, ())
-    sent(gall.at[c, a, pl.ds(0, (n - 1) * per)], gb_s, gb_r)
+    spread(
+        gall, ga_s, ga_r, gd_s, gd_r, [(0.1 * k, functools.partial(whole_piece, k)) for k in range(pieces)],
+        [(4.0, lambda: weight_lines(3))],
+    )
+    sent(rs1.at[:, others], r1_s, r1_r.at[0])
+    sent(rsb.at[:, others], rb_s, rb_r.at[0])
+    for p in range(n):
+        @pl.when(b == p)
+        def _():
+            sent(s1b.at[pl.ds(0, early - owned(p))], r2_s, r2_r.at[0])
+            if owned(p):
+                sent(gall.at[c, a, pl.ds(0, (n - 1) * owned(p))], gb_s, gb_r.at[0])
+
     arrived(gall.at[other], gd_s, gd_r)
 
-    sources = (x, x, None, None, None, None, around(x + 2, nx), around(x + 2, nx))
-    sides = (around(x - 1, nx), around(x + 1, nx))
-    rows = left.shape[1]
+    slots = ((0, 0), (0, 0), *(((1, nx - 1),) * 4), (2, 2), (2, 2))
+    arrived(left.at[pl.ds(1, nx - 1)], lx_s, lx_r)
+    rows = left.shape[2]
     left_done = jnp.zeros((n * rows, 2 * value_width), jnp.float32)
     for g in range(GROUPS):
-        columns = []
-        for i in range(2):
-            source = sides[i] if sources[g] is None else sources[g]
-            at = pl.multiple_of((source * 4 + CHUNK[g][i]) * ch, ch)
-            columns.append(left[:, :, pl.ds(at, ch)].reshape(n * rows, ch))
+        columns = [
+            left[slots[g][i], :, :, CHUNK[g][i] * ch : (CHUNK[g][i] + 1) * ch].reshape(n * rows, ch) for i in range(2)
+        ]
         grown = gall[:, :, g].reshape(2 * value_width, 2 * ch)
         left_done = left_done + dot(jnp.concatenate(columns, axis=1), grown, NT)
 
@@ -336,12 +399,13 @@
         else:
             total.append(squares)
 
-    spread(mall, ma_s, ma_r, md_s, md_r,
-           [(when, functools.partial(pass_on, index)) for index, when in enumerate((2.8, 6.6, 9.3))])
+    spread(
+        mall, ma_s, ma_r, md_s, md_r, [(0.35 * k, lambda: None) for k in range(ma_r.shape[1])],
+        [(4.7, lambda: weight_lines(4)), *((when, functools.partial(pass_on, index)) for index, when in enumerate((2.8, 6.6, 9.3)))],
+    )
     factor = clip_level * lax.rsqrt(total[0] / entries + epsilon)
     factor_out[...] = jnp.broadcast_to(factor[0:1, 0:1], factor_out.shape)
     grown_out[...] = grown_line[b]
-    weight_lines(4)
     arrived(wall.at[other], wd_s, wd_r)
     scale = factor[0:1, 0:1].reshape(1, 1, 1)
 
@@ -360,6 +424,7 @@
     lax.fori_loop(0, n, laid, 0)
     drained(gall, ga_s, ga_r.at[0, 0], gd_s, gd_r)
     drained(mall, ma_s, ma_r.at[0, 0], md_s, md_r)
+    sent(left.at[pl.ds(1, nx - 1)], lx_s, lx_r)
     drained(wall, wa_s, wa_r.at[0], wd_s, wd_r)
     for slots, send, recv, _, _, size in stages:
         sent(slots.at[pl.ds(0, size - 1)], send, recv)
@@ -398,20 +463,21 @@
         shapes((GROUPS, n, parts, pair), bf16),
         shapes((GROUPS, parts, pair), bf16),
         shapes((n, GROUPS // n, parts, pair), bf16),
+        shapes((LAST, n, parts, pair), bf16),
         shapes((2, n, GROUPS, parts, pair), bf16),
         shapes((2, n, n, rows, own_cols), f32),
         shapes((2, n, n, rows, own_cols), bf16),
         shapes((nx, *tile), f32),
         shapes((n, *tile), f32),
         shapes((2, *tile), f32),
-        shapes((n, *left_roots.shape), bf16),
+        shapes((nx, n, rows, own_cols), bf16),
         shapes((n, rows, own_cols), f32),
         shapes((n, rows, own_cols), f32),
     ]
     pieces = min(4, n)
     for received in (
-        (GROUPS - 2,), (GROUPS,), (), (GROUPS,), (), (), (n - 1, pieces), (), (n - 1, pieces), (),
-        (), (n - 1,), (), (), (), (), (), (),
+        (GROUPS - 2,), (GROUPS,), (), (GROUPS,), (GROUPS // n,), (LAST,), (GROUPS,), (n - 1, pieces), (), (n - 1, pieces), (),
+        (), (n - 1,), (), (), (), (), (), (), (),
     ):
         scratch += [dma, dma(received) if received else dma]
     inputs = [

time: 89.1 us -> 84.5 us (0.948)
  Pallas kernels: 86.3 us -> 81.6 us
    pallas_call x1, Pallas kernels: 86.3 us -> 81.6 us  [local(): pl.pallas_call(functools.partial(kernel, float(weight.size * n * n * 2 *...]
where the time goes in v4:
time: 84.5 us; the launch traced here: 84.3 us
  Pallas kernels  81.6 us (97%)
  local copies, waits for them, and re-layouts  1.33 us (2%)
    pallas_call x1, Pallas kernels, local(): pl.pallas_call(functools.partial(kernel, float(weight.size * n * n * 2 *...  81.6 us

profile of v4, /device:TPU:1, one launch (start us, length us, event | category | flops | bytes accessed | tf_op | source)
XLA Modules:
  0.0 84.3 jit_solution(18379817096115373226)
XLA Ops:
  0.6 0.0 copy-start.1
  0.6 0.0 copy-start
  0.7 81.6 %shard_map.147 = (f32[16,512]{1,0:T(8,128)S(1)}, f32[16,512]{1,0:T(8,128)S(1)}, bf16[8,8,2,16,512]{4,3,2,1,0:T(8,128)(2,1)S(1)}) custom-call(bf16[640,256]{1,0:T(8,128)(2,1)} %q1_in.1, bf16[640,256]{1,0:T(8,128)(2,1)} %k1_in.1, bf16[640,256]{1,0:T(8,128)(2,1)} %q2_in.1, bf16[640,256]{1,0:T(8,128)(2,1)} %k2_in.1, bf16[640,512]{1,0:T(8,128)(2,1)} %val_in.1, ...), custom_call_target="tpu_custom_call" | custom-call | tf_op jit(solution)/shard_map/pallas_call | solution.py:490
  82.3 0.0 copy-done.1
  82.3 0.0 copy-done
  82.3 0.6 multiply_subtract_fusion
  83.0 1.3 %copy.17 = bf16[2048,512]{1,0:T(8,128)(2,1)} copy(bf16[2048,512]{1,0:T(8,128)(2,1)S(1)} %bitcast.3) | data formatting | bytes 4194304
Async XLA Ops:
  0.6 81.7 %copy-start.1 = (f32[16,512]{1,0:T(8,128)S(1)}, f32[16,512]{1,0:T(8,128)}, u32[]{:S(2)}) copy-start(f32[16,512]{1,0:T(8,128)} %momentum_in.1) | copy-start | bytes 98308
  0.6 81.7 %copy-start = (f32[16,512]{1,0:T(8,128)S(1)}, f32[16,512]{1,0:T(8,128)}, u32[]{:S(2)}) copy-start(f32[16,512]{1,0:T(8,128)} %weight_in.1) | copy-start | bytes 98308

commit v5 on v4

--- a/solution.py
+++ b/solution.py
@@ -18,7 +18,7 @@
 step_rate = 0.1
 
 GROUPS = 8
-LAST = 3
+LAST = 4
 CHUNK = ((0, 1), (2, 3), (0, 2), (1, 3), (2, 0), (3, 1), (0, 2), (1, 3))
 NT = (((1,), (1,)), ((), ()))
 
@@ -254,8 +254,10 @@
             start(gsend.at[g, p], rs1.at[g, d], r1_s, r1_r.at[g], at_a(p))
         if g == 5:
             weight_lines(1)
-        if g >= 5:
-            finish(g - 5)
+        for ended in {4: (0, 1), 5: (2,), 6: (3,), 7: (4,)}.get(g, ()):
+            finish(ended)
+        for ended in {6: (0, 1), 7: (2,)}.get(g, ()):
+            own(ended)
     arrived(left.at[0, pl.ds(0, n - 1)], lb_s, lb_r)
     for d in range(1, nx):
         start(left.at[0], left.at[d], lx_s, lx_r, at_x(around(x + d, nx)))
@@ -267,19 +269,9 @@
     arrived(momentum.at[pl.ds(0, n - 1)], pb_s, pb_r)
     sent(left.at[0, pl.ds(0, n - 1)], lb_s, lb_r)
     loads["right"].wait()
-    finish(3)
-    finish(4)
-    own(0)
-    own(1)
-    own(2)
     finish(5)
     own(3)
     finish(6)
-    own(4)
-    finish(7)
-
-    weight_lines(2)
-
     def spread(buf, a_s, a_r, d_s, d_r, entries, extra):
         pieces = a_r.shape[1]
         count = buf.shape[2] // pieces
@@ -340,7 +332,7 @@
 
     spread(
         gall, ga_s, ga_r, gd_s, gd_r, [(0.1 * k, functools.partial(whole_piece, k)) for k in range(pieces)],
-        [(4.0, lambda: weight_lines(3))],
+        [(0.11, lambda: finish(7)), (0.12, lambda: weight_lines(2)), (4.0, lambda: weight_lines(3))],
     )
     sent(rs1.at[:, others], r1_s, r1_r.at[0])
     sent(rsb.at[:, others], rb_s, rb_r.at[0])

time: 84.5 us -> 82.6 us (0.978)
  Pallas kernels: 81.6 us -> 79.6 us
    pallas_call x1, Pallas kernels: 81.6 us -> 79.6 us  [local(): pl.pallas_call(functools.partial(kernel, float(weight.size * n * n * 2 *...]
where the time goes in v5:
time: 82.6 us; the launch traced here: 82.3 us
  Pallas kernels  79.6 us (96%)
  local copies, waits for them, and re-layouts  1.33 us (2%)
    pallas_call x1, Pallas kernels, local(): pl.pallas_call(functools.partial(kernel, float(weight.size * n * n * 2 *...  79.6 us

profile of v5, /device:TPU:1, one launch (start us, length us, event | category | flops | bytes accessed | tf_op | source)
XLA Modules:
  0.0 82.3 jit_solution(1179253960842004497)
XLA Ops:
  0.6 0.0 copy-start.1
  0.6 0.0 copy-start
  0.7 79.6 %shard_map.147 = (f32[16,512]{1,0:T(8,128)S(1)}, f32[16,512]{1,0:T(8,128)S(1)}, bf16[8,8,2,16,512]{4,3,2,1,0:T(8,128)(2,1)S(1)}) custom-call(bf16[640,256]{1,0:T(8,128)(2,1)} %q1_in.1, bf16[640,256]{1,0:T(8,128)(2,1)} %k1_in.1, bf16[640,256]{1,0:T(8,128)(2,1)} %q2_in.1, bf16[640,256]{1,0:T(8,128)(2,1)} %k2_in.1, bf16[640,512]{1,0:T(8,128)(2,1)} %val_in.1, ...), custom_call_target="tpu_custom_call" | custom-call | tf_op jit(solution)/shard_map/pallas_call | solution.py:482
  80.3 0.0 copy-done.1
  80.3 0.0 copy-done
  80.3 0.6 multiply_subtract_fusion
  81.0 1.3 %copy.17 = bf16[2048,512]{1,0:T(8,128)(2,1)} copy(bf16[2048,512]{1,0:T(8,128)(2,1)S(1)} %bitcast.3) | data formatting | bytes 4194304
Async XLA Ops:
  0.6 79.7 %copy-start.1 = (f32[16,512]{1,0:T(8,128)S(1)}, f32[16,512]{1,0:T(8,128)}, u32[]{:S(2)}) copy-start(f32[16,512]{1,0:T(8,128)} %momentum_in.1) | copy-start | bytes 98308
  0.6 79.7 %copy-start = (f32[16,512]{1,0:T(8,128)S(1)}, f32[16,512]{1,0:T(8,128)}, u32[]{:S(2)}) copy-start(f32[16,512]{1,0:T(8,128)} %weight_in.1) | copy-start | bytes 98308
